TPU v7x, 512 devices: a whole 4x4x16 slice. The times are simulated.
512 devices in a mesh: ep: 32 (over z, core), tp: 16 (over y, x).
Axes of the slice: x: 4, y: 4, z: 16, core: 2. Of those that a mesh axis runs over, the one named last changes fastest.
Arguments:
- reception_vectors: bfloat16 [4096, 2048], P('ep', 'tp'), may hold values from -6 to 6
- lookup_vectors: bfloat16 [4096, 2048], P('ep', 'tp'), may hold values from -0.75 to 0.75
- payload_vectors: bfloat16 [4096, 2048], P('ep', 'tp'), may hold values from -6 to 6
- fix_strength_signal: bfloat16 [4096, 2048], P('ep', 'tp'), may hold values from -5 to 5
- fade_signal_term: bfloat16 [4096, 2048], P('ep', 'tp'), may hold values from -8 to 8
- state_erasure: bfloat16 [4096, 2048], P('ep', 'tp'), may hold values from 0 to 1
- feature_speed_pairs: float32 [2, 2048], P(None, 'tp'), as said below
- subspace_scale_vector: float32 [2048], P('tp'), may hold values from 0.1 to 1.9
- subspace_merge_matrix: bfloat16 [2048, 4096], P(None, 'tp'), may hold values from -0.125 to 0.125
- specialist_entry_vectors: bfloat16 [2048, 4096], P('ep'), may hold values from -6 to 6
- specialist_entry_scale: float32 [4096], replicated, may hold values from 0.1 to 1.9
- specialist_picks: int32 [2048, 2], P('ep'), may hold values from 0 to 31, as said below
- dispatch_replica_share: float32 [2048, 2], P('ep'), may hold values from 0.2 to 1
- specialist_valve_matrix: bfloat16 [32, 4096, 2048], P('ep', None, 'tp'), may hold values from -0.09375 to 0.09375
- specialist_raising_matrix: bfloat16 [32, 4096, 2048], P('ep', None, 'tp'), may hold values from -0.09375 to 0.09375
- specialist_lowering_matrix: bfloat16 [32, 2048, 4096], P('ep', None, 'tp'), may hold values from -0.125 to 0.125
Outputs:
- sequence_blend_result: bfloat16 [4096, 4096], P('ep', 'tp')
- expert_out: bfloat16 [2048, 4096], P('ep', 'tp')
Inputs may be any that keep to these rules, and one draw needn't show every extreme that they name: `specialist_picks`: the two experts of a row differ and lie in one group, experts g * 8 to g * 8 + 7 for some g. Among the rows of one device (aligned blocks of 64 rows) no expert is named more than 6 times, and some expert exactly 6 times. `feature_speed_pairs`: Finite.
All inputs are finite; a program needn't handle non-finite values.
Results may differ from a plain program's by a relative error of at most 0.0071.
Values may be sent and summed in bfloat16 or wider, within the bound.
A program may use at most 64 MiB of HBM per device.

v0:
```python
import jax
import jax.numpy as jnp
from jax import lax
from jax.sharding import Mesh
from jax.sharding import PartitionSpec as P

HEAD = 64
GROUPS = 4
EP = ("ep_0", "ep_1")


highest = lax.Precision.HIGHEST
block_len = 16


def filled_with(shard, identity):
    return jax.tree.map(
        lambda a, e: jnp.broadcast_to(jnp.asarray(e, a.dtype), a.shape), shard, identity
    )


def carried_in(shard, axes, combine, identity):
    before = start = filled_with(shard, identity)
    running = shard
    for axis in reversed(axes):
        count, position = (lax.axis_size(axis), lax.axis_index(axis))
        pieces = jax.tree.map(lambda part: lax.all_gather(part, axis), running)
        inside, running = (start, start)
        for k in range(count):
            passed = k < position
            running = combine(running, jax.tree.map(lambda part: part[k], pieces))
            inside = jax.tree.map(lambda new, old: jnp.where(passed, new, old), running, inside)
        before = combine(inside, before)
    return before


def laid_out(blocks, dim):
    dims = list(blocks.shape[1:])
    dims[dim] *= blocks.shape[0]
    return jnp.moveaxis(blocks, 0, dim).reshape(dims)


def from_everyone(shard, axis):
    copies = jnp.broadcast_to(shard, (lax.axis_size(axis), *shard.shape))
    return lax.all_to_all(copies, axis, split_axis=0, concat_axis=0, tiled=True)


def gather_directly(shard, axis, dim):
    return laid_out(from_everyone(shard, axis), dim)


def product(left, right):
    return jnp.einsum("...ij,...jk->...ik", left, right, precision=highest)


def compose(earlier, later_pair):
    return (product(earlier[0], later_pair[0]), product(earlier[1], later_pair[0]) + later_pair[1])


def blend_sequence(
    reception_vectors,
    lookup_vectors,
    payload_vectors,
    fix_strength_signal,
    fade_signal_term,
    state_erasure,
    feature_speed_pairs,
    subspace_scale_vector,
    subspace_merge_matrix,
):
    span_len, channels = reception_vectors.shape
    head_count = channels // HEAD
    block_count = span_len // block_len
    fade_speed_exponent = jnp.exp(
        -jnp.exp(feature_speed_pairs[0] + fade_signal_term.astype(jnp.float32))
        - state_erasure.astype(jnp.float32)
    )
    learn_rate = jax.nn.sigmoid(fix_strength_signal.astype(jnp.float32) + feature_speed_pairs[1])
    key_heads = lookup_vectors.astype(jnp.float32).reshape(span_len, head_count, HEAD)
    key_unit = key_heads * lax.rsqrt(jnp.sum(key_heads * key_heads, axis=-1, keepdims=True) + 1e-06)

    def split_blocks(array):
        shaped = array.astype(jnp.float32).reshape(block_count, block_len, head_count, HEAD)
        return jnp.swapaxes(shaped, 0, 1)

    def advance(carry, inputs):
        state_mat, trans_mat = carry
        step_recept, step_decay, step_key, step_value, step_unit, step_learn = inputs
        removal = step_unit * step_learn
        state_hit = jnp.einsum("bhvk,bhk->bhv", state_mat, step_unit, precision=highest)
        state_mat = (
            state_mat * step_decay[:, :, None, :]
            - state_hit[..., None] * removal[:, :, None, :]
            + step_value[..., None] * step_key[:, :, None, :]
        )
        trans_hit = jnp.einsum("bhjk,bhk->bhj", trans_mat, step_unit, precision=highest)
        trans_mat = (
            trans_mat * step_decay[:, :, None, :] - trans_hit[..., None] * removal[:, :, None, :]
        )
        own_part = jnp.einsum("bhvk,bhk->bhv", state_mat, step_recept, precision=highest)
        carried = jnp.einsum("bhjk,bhk->bhj", trans_mat, step_recept, precision=highest)
        return ((state_mat, trans_mat), (own_part, carried))

    identity = jnp.broadcast_to(jnp.eye(HEAD, dtype=jnp.float32), (head_count, HEAD, HEAD))
    zero_mat = jnp.zeros((head_count, HEAD, HEAD), jnp.float32)
    start_carry = (
        jnp.zeros((block_count, head_count, HEAD, HEAD), jnp.float32),
        jnp.broadcast_to(identity, (block_count, head_count, HEAD, HEAD)),
    )
    step_inputs = (
        split_blocks(reception_vectors),
        split_blocks(fade_speed_exponent),
        split_blocks(key_heads),
        split_blocks(payload_vectors),
        split_blocks(key_unit),
        split_blocks(learn_rate),
    )
    block_pair, step_outputs = lax.scan(advance, start_carry, step_inputs)
    own_part, carried = step_outputs
    running_trans, running_state = lax.associative_scan(
        compose, (block_pair[1], block_pair[0]), axis=0
    )
    before_pair = carried_in(
        (running_trans[-1], running_state[-1]), EP, compose, (identity, zero_mat)
    )
    prior_trans = jnp.concatenate([identity[None], running_trans[:-1]], axis=0)
    prior_state = jnp.concatenate([zero_mat[None], running_state[:-1]], axis=0)
    entering = product(before_pair[1][None], prior_trans) + prior_state
    outputs = own_part + jnp.einsum("bhvk,tbhk->tbhv", entering, carried, precision=highest)
    outputs = jnp.swapaxes(outputs, 0, 1).reshape(span_len, head_count, HEAD)
    head_mean = jnp.mean(outputs, axis=-1, keepdims=True)
    centred = outputs - head_mean
    head_var = jnp.mean(centred * centred, axis=-1, keepdims=True)
    scaled = (
        centred * lax.rsqrt(head_var + 0.00064) * subspace_scale_vector.reshape(head_count, HEAD)
    )
    mixed_rows = scaled.reshape(span_len, channels).astype(jnp.bfloat16)
    return jnp.dot(
        gather_directly(mixed_rows, "tp", 1),
        subspace_merge_matrix,
        preferred_element_type=jnp.float32,
    ).astype(jnp.bfloat16)


def expert_layer(
    specialist_entry_vectors,
    specialist_entry_scale,
    specialist_picks,
    dispatch_replica_share,
    specialist_valve_matrix,
    specialist_raising_matrix,
    specialist_lowering_matrix,
):
    rows_here, model_width = specialist_entry_vectors.shape
    pairs = specialist_picks.shape[1]
    expert_count = lax.axis_size(EP) * specialist_valve_matrix.shape[0]
    per_group = expert_count // GROUPS
    busiest = per_group * max(1, 3 * rows_here // (8 * per_group))
    capacity = 2 * busiest // per_group
    widened = specialist_entry_vectors.astype(jnp.float32)
    normed = (
        widened
        * lax.rsqrt(jnp.mean(widened * widened, axis=-1, keepdims=True) + 1e-06)
        * specialist_entry_scale
    ).astype(jnp.bfloat16)
    flat_ids = specialist_picks.reshape(-1)
    onehot = (flat_ids[:, None] == jnp.arange(expert_count, dtype=jnp.int32)[None, :]).astype(
        jnp.int32
    )
    slot_rank = jnp.sum((jnp.cumsum(onehot, axis=0) - onehot) * onehot, axis=1)
    slot_index = flat_ids * capacity + slot_rank
    selected = jnp.arange(expert_count * capacity, dtype=jnp.int32)[:, None] == slot_index[None, :]
    selected = selected.reshape(expert_count * capacity, rows_here, pairs)
    placement_mat = jnp.any(selected, axis=-1).astype(jnp.bfloat16)
    combine_w = jnp.sum(selected.astype(jnp.float32) * dispatch_replica_share[None], axis=-1)
    send_rows = jnp.dot(placement_mat, normed, preferred_element_type=jnp.float32).astype(
        jnp.bfloat16
    )
    send_rows = send_rows.reshape(expert_count, capacity, model_width)
    arrived = lax.all_to_all(send_rows, EP, split_axis=0, concat_axis=0, tiled=True)
    sources, item_count, feature_count = arrived.shape
    flat_rows = arrived.reshape(sources * item_count, feature_count)
    gate_part = jnp.dot(flat_rows, specialist_valve_matrix[0], preferred_element_type=jnp.float32)
    up_part = jnp.dot(flat_rows, specialist_raising_matrix[0], preferred_element_type=jnp.float32)
    hidden = (jax.nn.silu(gate_part) * up_part).astype(jnp.bfloat16)
    weight_rows = specialist_lowering_matrix[0]
    result = jnp.dot(
        gather_directly(hidden, "tp", 1), weight_rows, preferred_element_type=jnp.float32
    ).astype(jnp.bfloat16)
    result = result.reshape(sources, item_count, specialist_lowering_matrix.shape[2])
    returned = lax.all_to_all(result, EP, split_axis=0, concat_axis=0, tiled=True)
    flat_back = returned.reshape(expert_count * capacity, returned.shape[2]).astype(jnp.float32)
    combined = jnp.einsum("st,sd->td", combine_w, flat_back, precision=highest)
    return combined.astype(jnp.bfloat16)


def body(
    reception_vectors,
    lookup_vectors,
    payload_vectors,
    fix_strength_signal,
    fade_signal_term,
    state_erasure,
    feature_speed_pairs,
    subspace_scale_vector,
    subspace_merge_matrix,
    specialist_entry_vectors,
    specialist_entry_scale,
    specialist_picks,
    dispatch_replica_share,
    specialist_valve_matrix,
    specialist_raising_matrix,
    specialist_lowering_matrix,
):
    sequence_blend_result = blend_sequence(
        reception_vectors,
        lookup_vectors,
        payload_vectors,
        fix_strength_signal,
        fade_signal_term,
        state_erasure,
        feature_speed_pairs,
        subspace_scale_vector,
        subspace_merge_matrix,
    )
    expert_out = expert_layer(
        specialist_entry_vectors,
        specialist_entry_scale,
        specialist_picks,
        dispatch_replica_share,
        specialist_valve_matrix,
        specialist_raising_matrix,
        specialist_lowering_matrix,
    )
    return (sequence_blend_result, expert_out)


def solution(mesh):
    torus = Mesh(mesh.devices.reshape(16, 2, mesh.shape["tp"]), ("ep_0", "ep_1", "tp"))
    placed = (
        P(EP, "tp"),
        P(EP, "tp"),
        P(EP, "tp"),
        P(EP, "tp"),
        P(EP, "tp"),
        P(EP, "tp"),
        P(None, "tp"),
        P("tp"),
        P(None, "tp"),
        P(EP, None),
        P(),
        P(EP, None),
        P(EP, None),
        P(EP, None, "tp"),
        P(EP, None, "tp"),
        P(EP, None, "tp"),
    )
    return jax.shard_map(
        body, mesh=torus, in_specs=placed, out_specs=(P(EP, "tp"), P(EP, "tp")), check_vma=False
    )
```

profile of v0, /device:TPU:1, one launch (start us, length us, event | category | flops | bytes accessed | tf_op | source)
XLA Modules:
  0.0 307.7 jit_solution(11666356045903290239)
XLA Ops:
  4.4 1.7 convolution_convert_fusion
  6.1 1.6 reshape.173
  7.7 16.9 %all-to-all-start.1 = ((bf16[32,6,4096]{2,1,0:T(8,128)(2,1)}), bf16[32,6,4096]{2,1,0:T(8,128)(2,1)}, u32[]{:S(2)}, u32[]{:S(2)}) async-start(bf16[32,6,4096]{2,1,0:T(8,128)(2,1)} %reshape.173), calls=%async_computation.1 | async-start | bytes 4194304 | tf_op jit(solution)/shard_map/all_to_all | solution.py:180
  26.2 118.8 %while.17 = (s32[]{:T(128)}, f32[8,2,64,64]{3,2,1,0:T(8,128)S(1)}, f32[8,2,64,64]{3,2,1,0:T(8,128)S(1)}, f32[16,8,2,64]{3,0,2,1:T(8,128)}, f32[16,8,2,64]{3,0,2,...) while((s32[]{:T(128)}, f32[8,2,64,64]{3,2,1,0:T(8,128)S(1)}, ...), condition=%wide.region_2.3_spmd.clone, body=%wide.region_1.2_spmd.clone.sunk | while | flops 3802115 | bytes 2224288 | solution.py:118
  29.7 1.5 dynamic_update_slice.12
  37.1 1.5 dynamic_update_slice.12
  51.9 1.5 dynamic_update_slice.12
  59.3 1.5 dynamic_update_slice.12
  74.2 1.5 dynamic_update_slice.12
  149.2 2.0 pad.48
  152.6 3.3 %pad.108 = f32[7,2,64,64]{3,2,1,0:T(8,128)} pad(f32[4,2,64,64]{3,2,1,0:T(8,128)S(1)} %add.207, f32[]{:T(128)} %constant.23.clone.1), padding=0_0_1x0_0_0x0_0_0x0_0_0 | pad | bytes 360452
  155.9 3.3 %pad.65 = f32[7,2,64,64]{3,2,1,0:T(8,128)} pad(f32[4,2,64,64]{3,2,1,0:T(8,128)S(1)} %pad_maximum_fusion.1, f32[]{:T(128)} %constant.23.clone.1), padding=0_0_1x0_0_0x0_0_0x0_0_0 | pad | bytes 360452 | tf_op jit(solution)/shard_map/slice | solution.py:127
  159.3 1.9 all_gather.18
  161.6 1.9 all_gather.21
  164.1 28.6 %all-gather = f32[32,64,64]{2,1,0:T(8,128)S(1)} all-gather(f32[2,64,64]{2,1,0:T(8,128)S(1)} %fusion.73), channel_id=2, replica_groups=mesh['ep_0'=16,'ep_1'=2,'tp'=16] {'ep_0'}, dimensions={0}, use_global_device_ids=true | all-gather | bytes 557056 | tf_op jit(solution)/shard_map/all_gather | solution.py:27
  192.7 26.8 %all-gather.1 = f32[32,64,64]{2,1,0:T(8,128)S(1)} all-gather(f32[2,64,64]{2,1,0:T(8,128)S(1)} %convolution_add_fusion.19), channel_id=3, replica_groups=mesh['ep_0'=16,'ep_1'=2,'tp'=16] {'ep_0'}, dimensions={0}, use_global_device_ids=true | all-gather | bytes 557056 | tf_op jit(solution)/shard_map/all_gather | solution.py:27
  225.4 2.6 reshape.174
  228.0 1.9 fusion.18
  231.5 6.8 %all-to-all-start.2 = ((bf16[16,192,128]{2,1,0:T(8,128)(2,1)}), bf16[16,192,128]{2,1,0:T(8,128)(2,1)S(1)}, u32[]{:S(2)}, u32[]{:S(2)}) async-start(bf16[16,192,128]{2,1,0:T(8,128)(2,1)} %broadcast_in_dim.49), calls=%async_computation.2 | async-start | bytes 1572864 | tf_op jit(solution)/shard_map/all_to_all | solution.py:45
  239.2 9.4 %all-to-all-done.2 = bf16[16,192,128]{2,1,0:T(8,128)(2,1)S(1)} async-done(((bf16[16,192,128]{2,1,0:T(8,128)(2,1)}), bf16[16,192,128]{2,1,0:T(8,128)(2,1)S(1)}, u32[]{:S(2)}, u32[]{:S(2)}) %all-to-all-start.2) | async-done | bytes 786464 | tf_op jit(solution)/shard_map/all_to_all | solution.py:45
  249.6 3.6 %all-to-all-start = ((bf16[16,128,128]{1,2,0:T(8,128)(2,1)}), bf16[16,128,128]{1,2,0:T(8,128)(2,1)S(1)}, u32[]{:S(2)}, u32[]{:S(2)}) async-start(bf16[16,128,128]{1,2,0:T(8,128)(2,1)} %broadcast_in_dim.48), calls=%async_computation | async-start | bytes 1048576 | tf_op jit(solution)/shard_map/all_to_all | solution.py:45
  254.2 10.5 %all-to-all-done = bf16[16,128,128]{1,2,0:T(8,128)(2,1)S(1)} async-done(((bf16[16,128,128]{1,2,0:T(8,128)(2,1)}), bf16[16,128,128]{1,2,0:T(8,128)(2,1)S(1)}, u32[]{:S(2)}, u32[]{:S(2)}) %all-to-all-start) | async-done | bytes 524320 | tf_op jit(solution)/shard_map/all_to_all | solution.py:45
  264.7 26.3 %all-to-all-start.3 = ((bf16[32,6,256]{2,1,0:T(8,128)(2,1)}), bf16[32,6,256]{2,1,0:T(8,128)(2,1)S(1)}, u32[]{:S(2)}, u32[]{:S(2)}) async-start(bf16[32,6,256]{2,1,0:T(8,128)(2,1)} %reshape.176), calls=%async_computation.3 | async-start | bytes 262144 | tf_op jit(solution)/shard_map/all_to_all | solution.py:191
  292.1 14.7 %all-to-all-done.3 = bf16[32,6,256]{2,1,0:T(8,128)(2,1)S(1)} async-done(((bf16[32,6,256]{2,1,0:T(8,128)(2,1)}), bf16[32,6,256]{2,1,0:T(8,128)(2,1)S(1)}, u32[]{:S(2)}, u32[]{:S(2)}) %all-to-all-start.3) | async-done | bytes 98336 | tf_op jit(solution)/shard_map/all_to_all | solution.py:191
  (320 shorter events, 134.2 us)
Async XLA Ops:
  0.6 252.5 %copy-start = (bf16[1,2048,256]{2,1,0:T(8,128)(2,1)S(1)}, bf16[1,2048,256]{2,1,0:T(8,128)(2,1)}, u32[]{:S(2)}) copy-start(bf16[1,2048,256]{2,1,0:T(8,128)(2,1)} %param.33) | copy-start | bytes 3145732
  7.7 17.0 %copy-start.12 = (bf16[128,128]{1,0:T(8,128)(2,1)S(1)}, bf16[128,128]{1,0:T(8,128)(2,1)}, u32[]{:S(2)}) copy-start(bf16[128,128]{1,0:T(8,128)(2,1)} %param.19) | copy-start | bytes 98308
  7.7 17.6 %copy-start.14 = (f32[2,128]{1,0:T(2,128)S(1)}, f32[2,128]{1,0:T(2,128)}, u32[]{:S(2)}) copy-start(f32[2,128]{1,0:T(2,128)} %param.24) | copy-start | bytes 3076
  7.7 17.6 %copy-start.7 = (bf16[128,128]{1,0:T(8,128)(2,1)S(1)}, bf16[128,128]{1,0:T(8,128)(2,1)}, u32[]{:S(2)}) copy-start(bf16[128,128]{1,0:T(8,128)(2,1)} %param.21) | copy-start | bytes 98308
  7.7 17.6 %copy-start.8 = (bf16[128,128]{1,0:T(8,128)(2,1)S(1)}, bf16[128,128]{1,0:T(8,128)(2,1)}, u32[]{:S(2)}) copy-start(bf16[128,128]{1,0:T(8,128)(2,1)} %param.23) | copy-start | bytes 98308
  7.7 17.6 %copy-start.9 = (bf16[128,128]{1,0:T(8,128)(2,1)S(1)}, bf16[128,128]{1,0:T(8,128)(2,1)}, u32[]{:S(2)}) copy-start(bf16[128,128]{1,0:T(8,128)(2,1)} %param.22) | copy-start | bytes 98308
  7.7 17.9 %copy-start.10 = (bf16[128,128]{1,0:T(8,128)(2,1)S(1)}, bf16[128,128]{1,0:T(8,128)(2,1)}, u32[]{:S(2)}) copy-start(bf16[128,128]{1,0:T(8,128)(2,1)} %param.20) | copy-start | bytes 98308
  7.7 18.1 %copy-start.11 = (bf16[128,128]{1,0:T(8,128)(2,1)S(1)}, bf16[128,128]{1,0:T(8,128)(2,1)}, u32[]{:S(2)}) copy-start(bf16[128,128]{1,0:T(8,128)(2,1)} %param.18) | copy-start | bytes 98308
  7.7 217.7 %all-to-all-start.1 = ((bf16[32,6,4096]{2,1,0:T(8,128)(2,1)}), bf16[32,6,4096]{2,1,0:T(8,128)(2,1)}, u32[]{:S(2)}, u32[]{:S(2)}) async-start(bf16[32,6,4096]{2,1,0:T(8,128)(2,1)} %reshape.173), calls=%async_computation.1 | async-start | bytes 4194304 | tf_op jit(solution)/shard_map/all_to_all | solution.py:180
  152.2 3.8 %copy-start.4 = (f32[1,2,64,64]{3,2,1,0:T(8,128)S(1)}, f32[1,2,64,64]{3,2,1,0:T(8,128)}, u32[]{:S(2)}) copy-start(f32[1,2,64,64]{3,2,1,0:T(8,128)} %slice.225) | copy-start | bytes 98308
  155.9 3.4 %slice-start = ((f32[7,2,64,64]{3,2,1,0:T(8,128)}), f32[1,2,64,64]{3,2,1,0:T(8,128)S(1)}, s32[]{:S(2)}) async-start(f32[7,2,64,64]{3,2,1,0:T(8,128)} %pad.108), calls=%async_computation.4 | async-start | bytes 131072 | tf_op jit(solution)/shard_map/slice | solution.py:124
  155.9 7.8 %copy-start.3 = (f32[3,2,64,64]{3,2,1,0:T(8,128)S(1)}, f32[3,2,64,64]{3,2,1,0:T(8,128)}, u32[]{:S(2)}) copy-start(f32[3,2,64,64]{3,2,1,0:T(8,128)} %fusion.34) | copy-start | bytes 294916
  221.5 1.8 copy-start.1
  223.4 0.9 copy-start.5
  223.4 1.0 copy-start.6
  228.0 1.9 copy-start.16
  230.4 8.7 %copy-start.15 = (f32[128]{0:T(128)S(1)}, f32[128]{0:T(128)}, u32[]{:S(2)}) copy-start(f32[128]{0:T(128)} %param.25) | copy-start | bytes 1540
  231.5 17.2 %all-to-all-start.2 = ((bf16[16,192,128]{2,1,0:T(8,128)(2,1)}), bf16[16,192,128]{2,1,0:T(8,128)(2,1)S(1)}, u32[]{:S(2)}, u32[]{:S(2)}) async-start(bf16[16,192,128]{2,1,0:T(8,128)(2,1)} %broadcast_in_dim.49), calls=%async_computation.2 | async-start | bytes 1572864 | tf_op jit(solution)/shard_map/all_to_all | solution.py:45
  249.6 15.1 %all-to-all-start = ((bf16[16,128,128]{1,2,0:T(8,128)(2,1)}), bf16[16,128,128]{1,2,0:T(8,128)(2,1)S(1)}, u32[]{:S(2)}, u32[]{:S(2)}) async-start(bf16[16,128,128]{1,2,0:T(8,128)(2,1)} %broadcast_in_dim.48), calls=%async_computation | async-start | bytes 1048576 | tf_op jit(solution)/shard_map/all_to_all | solution.py:45
  253.2 37.8 %copy-start.13 = (f32[64,2]{0,1:T(2,128)S(1)}, f32[64,2]{0,1:T(2,128)}, u32[]{:S(2)}) copy-start(f32[64,2]{0,1:T(2,128)} %param.30) | copy-start | bytes 1540
  253.2 38.0 %copy-start.2 = (bf16[2048,256]{1,0:T(8,128)(2,1)S(1)}, bf16[2048,256]{1,0:T(8,128)(2,1)}, u32[]{:S(2)}) copy-start(bf16[2048,256]{1,0:T(8,128)(2,1)} %param.26) | copy-start | bytes 3145732
  264.7 42.2 %all-to-all-start.3 = ((bf16[32,6,256]{2,1,0:T(8,128)(2,1)}), bf16[32,6,256]{2,1,0:T(8,128)(2,1)S(1)}, u32[]{:S(2)}, u32[]{:S(2)}) async-start(bf16[32,6,256]{2,1,0:T(8,128)(2,1)} %reshape.176), calls=%async_computation.3 | async-start | bytes 262144 | tf_op jit(solution)/shard_map/all_to_all | solution.py:191
where the time goes:
time: 310 us; the launch traced here: 308 us
  matrix products  74.8 us (24%)
  local copies, waits for them, and re-layouts  68.9 us (22%)
  blocking collectives  59.2 us (19%)
  starting transfers between devices  53.6 us (17%)
  waiting for transfers between devices  34.6 us (11%)
  other arithmetic  14.3 us (5%)
    all_gather x4, blocking collectives, carried_in(): pieces = jax.tree.map(lambda part: lax.all_gather(part, axis), running)  59.2 us
    dynamic_update_slice x32, local copies, waits for them, and re-layouts, blend_sequence(): block_pair, step_outputs = lax.scan(advance, start_carry, step_inputs)  48.4 us
    all_to_all x1, starting transfers between devices, expert_layer(): lax.all_to_all(result, EP, split_axis=0, concat_axis=0, tiled=True)  26.3 us
    all_to_all x2, waiting for transfers between devices, from_everyone(): return lax.all_to_all(copies, axis, split_axis=0, concat_axis=0, tiled=True)  19.9 us
    all_to_all x1, starting transfers between devices, expert_layer(): lax.all_to_all(send_rows, EP, split_axis=0, concat_axis=0, tiled=True)  16.9 us
    dot_general x16, matrix products, advance(): jnp.einsum('bhjk,bhk->bhj', trans_mat, step_unit, precision=highest)  14.8 us
    dot_general x16, matrix products, advance(): jnp.einsum('bhvk,bhk->bhv', state_mat, step_unit, precision=highest)  14.8 us
    dot_general x16, matrix products, advance(): jnp.einsum('bhjk,bhk->bhj', trans_mat, step_recept, precision=highest)  14.7 us
  transfers between devices with their start and end apart: 4, of which 3 were waited for; matrix products, arithmetic and copies ran while one was open for 46% of the time, Pallas kernels for 0%

commit v1 on v0

v1 whole, which is shorter than its diff:
```python
import jax
import jax.numpy as jnp
from jax import lax
from jax.experimental import pallas as pl
from jax.experimental.pallas import tpu as pltpu
from jax.sharding import PartitionSpec as P

HEAD = 64
SLOTS = 8
CAP = 6
F32, BF16 = jnp.float32, jnp.bfloat16
MESH = pl.DeviceIdType.MESH


def dot(a, b, ca, cb):
    return lax.dot_general(a, b, (((ca,), (cb,)), ((), ())), preferred_element_type=F32)


def split(a):
    high = a.astype(BF16)
    return high, (a - high.astype(F32)).astype(BF16)


def dot3(a, b, ca=1, cb=0):
    a_hi, a_lo = split(a)
    b_hi, b_lo = split(b)
    return dot(a_hi, b_hi, ca, cb) + (dot(a_hi, b_lo, ca, cb) + dot(a_lo, b_hi, ca, cb))


def sums_of(choice, parts):
    return sum(dot(choice, part, 1, 0) for part in parts)


def chosen(mask):
    return mask.astype(F32).astype(BF16)


def iota(shape, axis):
    return lax.broadcasted_iota(jnp.int32, shape, axis)


def per_head(array):
    first = iota(array.shape, 1) < HEAD
    low = jnp.sum(jnp.where(first, array, 0.0), axis=1, keepdims=True)
    high = jnp.sum(jnp.where(first, 0.0, array), axis=1, keepdims=True)
    return low, high


def by_head(low, high, shape):
    return jnp.where(iota(shape, 1) < HEAD, low, high)


def pair_matrices(recept, key, value, fix, fade, erase, speeds):
    n, c = key.shape
    recept, key, value = recept.astype(F32), key.astype(F32), value.astype(F32)
    log_decay = -jnp.exp(speeds[0:1] + fade.astype(F32)) - erase.astype(F32)
    log_decay = jnp.maximum(log_decay, -100.0)
    learn = 1.0 / (1.0 + jnp.exp(-(fix.astype(F32) + speeds[1:2])))
    first = iota((n, c), 1) < HEAD
    unit = key * lax.rsqrt(by_head(*per_head(key * key), (n, c)) + 1e-6)
    removal = unit * learn

    part_a = log_decay.astype(BF16)
    rest = log_decay - part_a.astype(F32)
    part_b = rest.astype(BF16)
    part_c = (rest - part_b.astype(F32)).astype(BF16)
    parts = (part_a, part_b, part_c)

    row, col, pos = iota((n, n), 0), iota((n, n), 1), iota((n, c), 0)
    differ = row ^ col

    def both_heads(array):
        return jnp.concatenate([jnp.where(first, array, 0.0), jnp.where(first, 0.0, array)], 0)

    total = jnp.zeros((4 * n, 2 * n), F32)
    size = 1
    while size < n:
        later = (row & size) != 0
        mid = row & ~(size - 1)
        key_rows = chosen(later & (col >= mid) & (col < row))
        read_rows = chosen(later & (col >= mid) & (col <= row))
        end = (row | (size - 1)) + 1
        write_rows = chosen(jnp.logical_not(later) & (col > row) & (col < end))
        is_later = (pos & size) != 0
        key_in = jnp.where(is_later, unit * jnp.exp(sums_of(key_rows, parts)), 0.0)
        read_in = jnp.where(is_later, recept * jnp.exp(sums_of(read_rows, parts)), 0.0)
        fading = jnp.where(is_later, 0.0, jnp.exp(sums_of(write_rows, parts)))
        left = jnp.concatenate([both_heads(key_in), both_heads(read_in)], 0)
        right = jnp.concatenate([removal * fading, key * fading], 0)
        found = dot3(left, right, 1, 1)
        level = (differ >= size) & (differ < 2 * size) & (row > col)
        level = jnp.concatenate([level, level], 1)
        level = jnp.concatenate([level, level, level, level], 0)
        total = jnp.where(level, found, total)
        size *= 2
    return recept, key, value, unit, removal, log_decay, parts, total


def pair_results(recept, key, value, unit, removal, log_decay, parts, total):
    n, c = key.shape
    row, col = iota((n, n), 0), iota((n, n), 1)
    differ = row ^ col
    first = iota((n, c), 1) < HEAD

    def pick_lanes(pair):
        return jnp.where(first, pair[0], pair[1])

    eye = row == col
    own_write = per_head(recept * key)
    own_removal = per_head(recept * removal)
    heads = range(2)
    solve_mat = [total[h * n : (h + 1) * n, :n] for h in heads]
    solve_val = [total[h * n : (h + 1) * n, n:] for h in heads]
    read_rem = [jnp.where(eye, own_removal[h], total[(2 + h) * n : (3 + h) * n, :n]) for h in heads]
    read_val = [jnp.where(eye, own_write[h], total[(2 + h) * n : (3 + h) * n, n:]) for h in heads]

    below = row > col
    inverse = [
        jnp.where(eye, 1.0, jnp.where((differ == 1) & below, -solve_mat[h], 0.0)) for h in heads
    ]
    size = 2
    while size < n:
        level = (differ >= size) & (differ < 2 * size) & below
        inner = [dot3(jnp.where(level, solve_mat[h], 0.0), inverse[h]) for h in heads]
        inverse = [inverse[h] - dot3(inverse[h], inner[h]) for h in heads]
        size *= 2

    before = sums_of(chosen(col < row), parts)
    upto = before + log_decay
    after = sums_of(chosen(col > row), parts)
    key_start = unit * jnp.exp(before)
    read_start = recept * jnp.exp(upto)
    to_end = jnp.exp(after)
    whole = jnp.exp(upto[n - 1 : n])

    hit_val = pick_lanes([dot3(solve_val[h], value) for h in heads])
    both = jnp.concatenate([key_start, hit_val], 1)
    hits = [dot3(inverse[h], both) for h in heads]
    both = jnp.concatenate(
        [pick_lanes([hits[h][:, :c] for h in heads]), pick_lanes([hits[h][:, c:] for h in heads])],
        1,
    )
    taken = [dot3(read_rem[h], both) for h in heads]
    carried = read_start - pick_lanes([taken[h][:, :c] for h in heads])
    own_out = pick_lanes([dot3(read_val[h], value) - taken[h][:, c:] for h in heads])

    removed = dot3(removal * to_end, both, 0, 0)
    written = dot3(key * to_end, value, 0, 0)
    trans = jnp.where(eye, whole, 0.0) - removed[:, :c]
    state = written - removed[:, c:]
    pair = jnp.concatenate(
        [
            jnp.concatenate([trans[:HEAD, :HEAD], state[:HEAD, :HEAD]], 1),
            jnp.concatenate([trans[HEAD:, HEAD:], state[HEAD:, HEAD:]], 1),
        ],
        0,
    )
    return carried, own_out, pair


def compose(earlier, later):
    right = iota(later.shape, 1) >= HEAD
    return dot3(later[:, :HEAD], earlier) + jnp.where(right, later, 0.0)


class Gather:
    def __init__(self, buf, send_sem, recv_sem, place, ny, nx):
        self.buf, self.send_sem, self.recv_sem = buf, send_sem, recv_sem
        self.ep, self.y, self.x = place
        self.ny, self.nx = ny, nx
        self.half = buf.shape[2] // 2

    def block(self, half, phase, step, begin, count):
        rows = pl.ds(half * self.half + begin, count)
        if (half + phase) % 2 == 0:
            at = lax.rem(self.x + step + self.nx, self.nx)
            if phase == 0:
                return self.buf.at[self.y, at, rows]
            return self.buf.at[:, at, rows]
        at = lax.rem(self.y + step + self.ny, self.ny)
        if phase == 0:
            return self.buf.at[at, self.x, rows]
        return self.buf.at[at, :, rows]

    def other(self, half, phase, step):
        if (half + phase) % 2 == 0:
            x, y = lax.rem(self.x + step + self.nx, self.nx), self.y
        else:
            x, y = self.x, lax.rem(self.y + step + self.ny, self.ny)
        return {"ep": self.ep, "tp": y * self.nx + x}

    def sent(self, half, phase, kind):
        part = self.half // 2
        step, begin, count, to = (
            (0, 0, 2 * part, 1),
            (0, 0, 2 * part, -1),
            (-1, 0, part, 1),
            (1, part, part, -1),
        )[kind]
        block = self.block(half, phase, step, begin, count)
        at = (half * 2 + phase) * 4 + kind
        return pltpu.make_async_remote_copy(
            src_ref=block,
            dst_ref=block,
            send_sem=self.send_sem.at[at],
            recv_sem=self.recv_sem.at[at],
            device_id=self.other(half, phase, to),
            device_id_type=MESH,
        )

    def arrived(self, half, phase, kind):
        part = self.half // 2
        step, begin, count = (
            (-1, 0, 2 * part),
            (1, 0, 2 * part),
            (-2, 0, part),
            (2, part, part),
        )[kind]
        block = self.block(half, phase, step, begin, count)
        at = (half * 2 + phase) * 4 + kind
        pltpu.make_async_copy(block, block, self.recv_sem.at[at]).wait()

    def start(self, half, phase):
        self.sent(half, phase, 0).start()
        self.sent(half, phase, 1).start()

    def forward(self, half, phase):
        self.arrived(half, phase, 0)
        self.sent(half, phase, 2).start()
        self.arrived(half, phase, 1)
        self.sent(half, phase, 3).start()

    def finish(self, half, phase):
        self.arrived(half, phase, 2)
        self.arrived(half, phase, 3)

    def drain(self):
        for half in range(2):
            for phase in range(2):
                for kind in range(4):
                    self.sent(half, phase, kind).wait_send()


def wait_for(ref, sem):
    pltpu.make_async_copy(ref, ref, sem).wait()


def kernel(
    n_ep,
    n_y,
    n_x,
    group,
    recept_ref,
    key_ref,
    value_ref,
    fix_ref,
    fade_ref,
    erase_ref,
    speeds_ref,
    gain_ref,
    merge_hbm,
    rows_ref,
    scale_ref,
    picks_ref,
    share_ref,
    gate_hbm,
    up_hbm,
    down_hbm,
    blend_out,
    expert_out,
    merge_ref,
    gate_up_ref,
    down_ref,
    send_buf,
    recv_buf,
    rows_all,
    hidden_all,
    back_buf,
    ret_buf,
    mixed_all,
    pair_buf,
    pair_in,
    chip_pairs,
    group_pairs,
    state_out,
    state_in,
    load_sem,
    ep_send,
    ep_recv,
    x_send,
    x_recv,
    h_send,
    h_recv,
    m_send,
    m_recv,
    scan_send,
    scan_recv,
):
    ep, tp = lax.axis_index("ep"), lax.axis_index("tp")
    core, z = lax.rem(ep, 2), ep // 2
    y, x = tp // n_x, lax.rem(tp, n_x)
    place = lax.rem(z, group)
    n_group = n_ep // 2 // group
    mine = z // group
    partner = ep + 1 - 2 * core
    n, c = key_ref.shape
    n_rows = rows_ref.shape[0]
    lanes = send_buf.shape[2]
    slots = n_ep * SLOTS
    depth = gate_hbm.shape[1]

    loads = [
        pltpu.make_async_copy(gate_hbm, gate_up_ref.at[:, pl.ds(0, depth)], load_sem.at[0]),
        pltpu.make_async_copy(up_hbm, gate_up_ref.at[:, pl.ds(depth, depth)], load_sem.at[1]),
        pltpu.make_async_copy(down_hbm, down_ref, load_sem.at[2]),
        pltpu.make_async_copy(merge_hbm, merge_ref, load_sem.at[3]),
    ]
    for load in loads:
        load.start()

    barrier = pltpu.get_barrier_semaphore()

    def greet(step, carry):
        pl.semaphore_signal(
            barrier,
            inc=1,
            device_id={"ep": lax.rem(ep + step, n_ep), "tp": tp},
            device_id_type=MESH,
        )
        return carry

    lax.fori_loop(1, n_ep, greet, 0)
    for step in (1, -1):
        for other in (
            y * n_x + lax.rem(x + step + n_x, n_x),
            lax.rem(y + step + n_y, n_y) * n_x + x,
        ):
            pl.semaphore_signal(
                barrier, inc=1, device_id={"ep": ep, "tp": other}, device_id_type=MESH
            )

    widened = rows_ref[...].astype(F32)
    strength = lax.rsqrt(jnp.mean(widened * widened, axis=1, keepdims=True) + 1e-6)
    own = pl.ds(pl.multiple_of(tp * lanes, 128), lanes)
    normed = (rows_ref[:, own].astype(F32) * strength * scale_ref[:, own]).astype(BF16)
    slot = iota((n_rows, slots), 1)
    expert = slot // SLOTS
    named = [picks_ref[:, k : k + 1] == expert for k in range(2)]
    either = named[0] | named[1]
    earlier = chosen(iota((n_rows, n_rows), 1) < iota((n_rows, n_rows), 0))
    rank = dot(earlier, chosen(either), 1, 0)
    taken = either & (rank == lax.rem(slot, SLOTS).astype(F32))
    weight = jnp.where(taken & named[0], share_ref[:, 0:1], 0.0) + jnp.where(
        taken & named[1], share_ref[:, 1:2], 0.0
    )
    send_buf[...] = dot(chosen(taken), normed, 0, 0).reshape(n_ep, SLOTS, lanes).astype(BF16)

    matrices = pair_matrices(
        recept_ref[...],
        key_ref[...],
        value_ref[...],
        fix_ref[...],
        fade_ref[...],
        erase_ref[...],
        speeds_ref[...],
    )

    pl.semaphore_wait(barrier, n_ep - 1 + 4)

    def ep_copy(src, dst, step, at):
        other = lax.rem(ep + step, n_ep)
        return pltpu.make_async_remote_copy(
            src_ref=src.at[other],
            dst_ref=dst.at[ep],
            send_sem=ep_send.at[at],
            recv_sem=ep_recv.at[at],
            device_id={"ep": other, "tp": tp},
            device_id_type=MESH,
        )

    def ep_exchange(src, dst, at):
        def send(step, carry):
            ep_copy(src, dst, step, at).start()
            return carry

        lax.fori_loop(1, n_ep, send, 0)
        dst[ep] = src[ep]

    ep_exchange(send_buf, recv_buf, 0)

    carried, own_out, pair = pair_results(*matrices)
    pair_buf[...] = pair

    def scan_copy(src, dst, device, at):
        return pltpu.make_async_remote_copy(
            src_ref=src,
            dst_ref=dst,
            send_sem=scan_send.at[at],
            recv_sem=scan_recv.at[at],
            device_id={"ep": device, "tp": tp},
            device_id_type=MESH,
        )

    theirs = pair_buf.at[pl.ds(pl.multiple_of(HEAD * (1 - core), HEAD), HEAD)]
    swap = scan_copy(theirs, pair_in, partner, 0)
    swap.start()
    swap.wait_recv()
    own_pair = pair_buf[pl.ds(pl.multiple_of(HEAD * core, HEAD), HEAD), :]
    other_pair = pair_in[...]
    even = core == 0
    pair_0 = jnp.where(even, own_pair, other_pair)
    pair_1 = jnp.where(even, other_pair, own_pair)
    chip_pairs[place] = compose(pair_0, pair_1)
    local = []
    for step in range(1, group):
        at = lax.rem(place + step, group)
        local.append(
            scan_copy(
                chip_pairs.at[place],
                chip_pairs.at[place],
                2 * (mine * group + at) + core,
                step,
            )
        )
        local[-1].start()
    for step in range(1, group):
        at = lax.rem(place - step + group, group)
        wait_for(chip_pairs.at[at], scan_recv.at[step])
    prefix = [chip_pairs[0]]
    for at in range(1, group):
        prefix.append(compose(prefix[-1], chip_pairs[at]))
    ident = jnp.where(iota((HEAD, c), 0) == iota((HEAD, c), 1), 1.0, 0.0)
    inside = ident
    for at in range(group - 1):
        inside = jnp.where(place == at + 1, prefix[at], inside)
    group_pairs[mine] = prefix[-1]

    def group_copy(step):
        return scan_copy(
            group_pairs.at[mine],
            group_pairs.at[mine],
            2 * ((mine + step) * group + place) + core,
            group + step - 1,
        )

    for step in range(1, n_group):

        @pl.when(mine + step < n_group)
        def _(step=step):
            group_copy(step).start()

    wait_for(recv_buf.at[pl.ds(0, n_ep - 1)], ep_recv.at[0])
    packed, spread = iota((n_ep * CAP, slots), 0), iota((n_ep * CAP, slots), 1)
    inner = lax.rem(spread, SLOTS)
    pack = chosen((inner < CAP) & (spread // SLOTS * CAP + inner == packed))
    arrived = recv_buf[...].astype(F32).reshape(slots, lanes).astype(BF16)
    rows_all[y, x] = dot(pack, arrived, 1, 0).astype(BF16)

    spot = (ep, y, x)
    xs = Gather(rows_all, x_send, x_recv, spot, n_y, n_x)
    hs = Gather(hidden_all, h_send, h_recv, spot, n_y, n_x)
    ms = Gather(mixed_all, m_send, m_recv, spot, n_y, n_x)
    both = (0, 1)
    for half in both:
        xs.start(half, 0)
    for half in both:
        xs.forward(half, 0)
    for half in both:
        xs.finish(half, 0)
        xs.start(half, 1)

    for step in range(1, n_group):

        @pl.when(mine >= step)
        def _(step=step):
            wait_for(group_pairs.at[mine - step], scan_recv.at[group + step - 1])

    state = jnp.zeros((HEAD, c), F32)
    for at in range(n_group - 1):
        state = jnp.where(at < mine, compose(state, group_pairs[at]), state)
    state_0 = compose(state, inside)
    state_1 = compose(state_0, pair_0)
    state_out[...] = jnp.where(even, state_1, state_0)
    give = scan_copy(state_out, state_in, partner, group + n_group - 1)
    give.start()
    state_own = jnp.where(even, state_0, state_1)

    for half in both:
        xs.forward(half, 1)

    give.wait_recv()
    state_other = state_in[...]
    state_a = jnp.where(even, state_own, state_other)
    state_b = jnp.where(even, state_other, state_own)
    right = iota((HEAD, c), 1) >= HEAD
    entering = jnp.concatenate(
        [
            jnp.concatenate([state_a[:, HEAD:], jnp.zeros((HEAD, HEAD), F32)], 1),
            jnp.where(right, state_b, 0.0),
        ],
        0,
    )
    out = dot3(carried, entering) + own_out
    mean = by_head(*per_head(out), (n, c)) * (1.0 / HEAD)
    centred = out - mean
    spread_of = by_head(*per_head(centred * centred), (n, c)) * (1.0 / HEAD)
    mixed = centred * lax.rsqrt(spread_of + 0.00064) * gain_ref[...]
    mixed_all[y, x] = mixed.astype(BF16)
    for half in both:
        ms.start(half, 0)

    for half in both:
        xs.finish(half, 1)
    for load in loads[:2]:
        load.wait()

    total = jnp.zeros((n_ep * CAP, 2 * depth), F32)
    for j in range(n_y * n_x):
        total = total + dot(
            rows_all[j // n_x, j % n_x], gate_up_ref[j * lanes : (j + 1) * lanes, :], 1, 0
        )
    gated, raised = total[:, :depth], total[:, depth:]
    hidden_all[y, x] = (gated / (1.0 + jnp.exp(-gated)) * raised).astype(BF16)
    for half in both:
        hs.start(half, 0)
    for half in both:
        ms.forward(half, 0)
    for half in both:
        hs.forward(half, 0)
    for half in both:
        hs.finish(half, 0)
        hs.start(half, 1)
    for half in both:
        ms.finish(half, 0)
        ms.start(half, 1)
    for half in both:
        hs.forward(half, 1)
    for half in both:
        ms.forward(half, 1)
    for half in both:
        hs.finish(half, 1)
    loads[2].wait()
    result = jnp.zeros((n_ep * CAP, lanes), F32)
    for j in range(n_y * n_x):
        result = result + dot(
            hidden_all[j // n_x, j % n_x], down_ref[j * depth : (j + 1) * depth, :], 1, 0
        )
    back_buf[...] = dot(pack, result.astype(BF16), 0, 0).reshape(n_ep, SLOTS, lanes).astype(BF16)
    ep_exchange(back_buf, ret_buf, 1)

    for half in both:
        ms.finish(half, 1)
    loads[3].wait()
    blend = jnp.zeros(blend_out.shape, F32)
    for j in range(n_y * n_x):
        blend = blend + dot(mixed_all[j // n_x, j % n_x], merge_ref[j * c : (j + 1) * c, :], 1, 0)
    blend_out[...] = blend.astype(BF16)

    for gather in (xs, hs, ms):
        gather.drain()
    swap.wait_send()
    give.wait_send()
    for copy in local:
        copy.wait_send()
    for step in range(1, n_group):

        @pl.when(mine + step < n_group)
        def _(step=step):
            group_copy(step).wait_send()

    wait_for(send_buf.at[pl.ds(0, n_ep - 1)], ep_send.at[0])
    wait_for(ret_buf.at[pl.ds(0, n_ep - 1)], ep_recv.at[1])
    returned = ret_buf[...].astype(F32).reshape(slots, lanes).astype(BF16)
    w_hi, w_lo = split(weight)
    expert_out[...] = (dot(w_hi, returned, 1, 0) + dot(w_lo, returned, 1, 0)).astype(BF16)
    wait_for(back_buf.at[pl.ds(0, n_ep - 1)], ep_send.at[1])


def body(
    n_ep,
    n_y,
    n_x,
    group,
    recept,
    key,
    value,
    fix,
    fade,
    erase,
    speeds,
    gain,
    merge,
    rows,
    scale,
    picks,
    share,
    gate,
    up,
    down,
):
    n, c = key.shape
    n_rows, width = rows.shape
    lanes = down.shape[2]
    depth = gate.shape[2]
    slots = n_ep * CAP
    n_group = n_ep // 2 // group
    scans = group + n_group
    vmem, hbm = pl.BlockSpec(memory_space=pltpu.VMEM), pl.BlockSpec(memory_space=pltpu.HBM)
    dma = pltpu.SemaphoreType.DMA
    return pl.pallas_call(
        lambda *refs: kernel(n_ep, n_y, n_x, group, *refs),
        out_shape=(
            jax.ShapeDtypeStruct((n, merge.shape[1]), BF16),
            jax.ShapeDtypeStruct((n_rows, lanes), BF16),
        ),
        in_specs=[vmem] * 8 + [hbm] + [vmem] * 4 + [hbm] * 3,
        out_specs=(vmem, vmem),
        scratch_shapes=[
            pltpu.VMEM(merge.shape, BF16),
            pltpu.VMEM((width, 2 * depth), BF16),
            pltpu.VMEM(down.shape[1:], BF16),
            pltpu.VMEM((n_ep, SLOTS, lanes), BF16),
            pltpu.VMEM((n_ep, SLOTS, lanes), BF16),
            pltpu.VMEM((n_y, n_x, slots, lanes), BF16),
            pltpu.VMEM((n_y, n_x, slots, depth), BF16),
            pltpu.VMEM((n_ep, SLOTS, lanes), BF16),
            pltpu.VMEM((n_ep, SLOTS, lanes), BF16),
            pltpu.VMEM((n_y, n_x, n, c), BF16),
            pltpu.VMEM((n, c), F32),
            pltpu.VMEM((HEAD, c), F32),
            pltpu.VMEM((group, HEAD, c), F32),
            pltpu.VMEM((n_group, HEAD, c), F32),
            pltpu.VMEM((HEAD, c), F32),
            pltpu.VMEM((HEAD, c), F32),
            dma((4,)),
            dma((2,)),
            dma((2,)),
            dma((16,)),
            dma((16,)),
            dma((16,)),
            dma((16,)),
            dma((16,)),
            dma((16,)),
            dma((scans,)),
            dma((scans,)),
        ],
        compiler_params=pltpu.CompilerParams(
            collective_id=0, has_side_effects=True, vmem_limit_bytes=56 << 20
        ),
    )(
        recept,
        key,
        value,
        fix,
        fade,
        erase,
        speeds,
        gain.reshape(1, c),
        merge,
        rows,
        scale.reshape(1, width),
        picks,
        share,
        gate[0],
        up[0],
        down[0],
    )


def solution(mesh):
    n_ep, n_tp = mesh.shape["ep"], mesh.shape["tp"]
    n_x = 4
    group = 4
    placed = (
        *(P("ep", "tp"),) * 6,
        P(None, "tp"),
        P("tp"),
        P(None, "tp"),
        P("ep", None),
        P(),
        P("ep", None),
        P("ep", None),
        *(P("ep", None, "tp"),) * 3,
    )
    return jax.shard_map(
        lambda *args: body(n_ep, n_tp // n_x, n_x, group, *args),
        mesh=mesh,
        in_specs=placed,
        out_specs=(P("ep", "tp"), P("ep", "tp")),
        check_vma=False,
    )
```

time: 310 us -> 80.2 us (0.26)
  Pallas kernels: 0 us -> 75.2 us
  matrix products: 74.8 us -> 0 us
  local copies, waits for them, and re-layouts: 68.9 us -> 4.19 us
  blocking collectives: 59.2 us -> 0 us
  starting transfers between devices: 53.6 us -> 0 us
  waiting for transfers between devices: 34.6 us -> 0 us
  other arithmetic: 14.3 us -> 0 us
    pallas_call x0 -> x1, Pallas kernels: none -> 75.2 us  [body(): pl.pallas_call(lambda *refs: kernel(n_ep, n_y, n_x, group, *refs), out_sh...]
    dot_general x105 -> x0, matrix products: 74.8 us -> none  [the longest x16 14.8 us: advance(): jnp.einsum('bhjk,bhk->bhj', trans_mat, step_unit, precision=highest)]
    all_gather x4 -> x0, blocking collectives: 59.2 us -> none  [carried_in(): pieces = jax.tree.map(lambda part: lax.all_gather(part, axis), running)]
    all_to_all x4 -> x0, starting transfers between devices: 53.6 us -> none  [the longest x1 26.3 us: expert_layer(): lax.all_to_all(result, EP, split_axis=0, concat_axis=0, tiled=True)]
    dynamic_update_slice x32 -> x0, local copies, waits for them, and re-layouts: 48.4 us -> none  [blend_sequence(): block_pair, step_outputs = lax.scan(advance, start_carry, step_inputs)]
    all_to_all x4 -> x0, waiting for transfers between devices: 34.6 us -> none  [the longest x2 19.9 us: from_everyone(): return lax.all_to_all(copies, axis, split_axis=0, concat_axis=0, tiled=True)]
    sub x16 -> x0, other arithmetic: 9.65 us -> none  [advance(): trans_mat * step_decay[:, :, None, :]]
    reshape x7 -> x0, local copies, waits for them, and re-layouts: 5.26 us -> none  [the longest x1 2.55 us: expert_layer(): flat_rows = arrived.reshape(sources * item_count, feature_count)]
  transfers between devices with their start and end apart: 4 -> 0, of which waited for: 3 -> 0; matrix products, arithmetic and copies ran while one was open for 46% -> 0% of each run, Pallas kernels for 0% -> 0%
where the time goes in v1:
time: 80.2 us; the launch traced here: 80 us
  Pallas kernels  75.2 us (94%)
  local copies, waits for them, and re-layouts  4.19 us (5%)
    pallas_call x1, Pallas kernels, body(): pl.pallas_call(lambda *refs: kernel(n_ep, n_y, n_x, group, *refs), out_sh...  75.2 us
    unnamed x10, local copies, waits for them, and re-layouts  4.19 us

profile of v1, /device:TPU:1, one launch (start us, length us, event | category | flops | bytes accessed | tf_op | source)
XLA Modules:
  0.0 80.0 jit_solution(3634528893669495012)
XLA Ops:
  0.6 0.0 copy-start.1
  0.6 0.7 copy-done.1
  1.3 0.0 copy-start.2
  1.3 0.7 copy.18.refs_11_
  2.0 0.0 copy-done.2
  2.0 0.7 copy.19.refs_12_
  2.7 75.2 %shard_map.167 = (bf16[128,256]{1,0:T(8,128)(2,1)}, bf16[64,256]{1,0:T(8,128)(2,1)}) custom-call(bf16[128,128]{1,0:T(8,128)(2,1)} %refs_0_.1, bf16[128,128]{1,0:T(8,128)(2,1)} %refs_1_.1, bf16[128,128]{1,0:T(8,128)(2,1)} %refs_2_.1, bf16[128,128]{1,0:T(8,128)(2,1)} %refs_3_.1, bf16[128,128]{1,0:T(8,128)(2,1)} %refs_4_.1, bf16[128,128]{1,0:T(8,128)(2,1)} %refs_5_.1, ...), custom_call_target="tpu_custom_call" | custom-call | tf_op jit(solution)/shard_map/pallas_call | solution.py:610
  77.9 0.0 copy-start
  77.9 1.5 %copy.22 = bf16[128,256]{1,0:T(8,128)(2,1)} copy(bf16[128,256]{1,0:T(8,128)(2,1)} %get-tuple-element.4) | data formatting | bytes 131072
  79.4 0.0 copy-done
  79.4 0.6 copy.23
Async XLA Ops:
  0.6 0.7 copy-start.1
  1.3 0.7 copy-start.2
  77.9 1.5 %copy-start = (bf16[64,256]{1,0:T(8,128)(2,1)S(1)}, bf16[64,256]{1,0:T(8,128)(2,1)}, u32[]{:S(2)}) copy-start(bf16[64,256]{1,0:T(8,128)(2,1)} %get-tuple-element.5) | copy-start | bytes 98308

commit v2 on v1

--- a/solution.py
+++ b/solution.py
@@ -8,6 +8,7 @@
 HEAD = 64
 SLOTS = 8
 CAP = 6
+CHUNKS = 2
 F32, BF16 = jnp.float32, jnp.bfloat16
 MESH = pl.DeviceIdType.MESH
 
@@ -163,15 +164,15 @@
     return dot3(later[:, :HEAD], earlier) + jnp.where(right, later, 0.0)
 
 
-class Gather:
+class TwoPhase:
     def __init__(self, buf, send_sem, recv_sem, place, ny, nx):
         self.buf, self.send_sem, self.recv_sem = buf, send_sem, recv_sem
         self.ep, self.y, self.x = place
         self.ny, self.nx = ny, nx
         self.half = buf.shape[2] // 2
 
-    def block(self, half, phase, step, begin, count):
-        rows = pl.ds(half * self.half + begin, count)
+    def block(self, half, phase, step):
+        rows = pl.ds(half * self.half, self.half)
         if (half + phase) % 2 == 0:
             at = lax.rem(self.x + step + self.nx, self.nx)
             if phase == 0:
@@ -182,63 +183,94 @@
             return self.buf.at[at, self.x, rows]
         return self.buf.at[at, :, rows]
 
-    def other(self, half, phase, step):
+    def steps(self, half, phase):
+        count = self.nx if (half + phase) % 2 == 0 else self.ny
+        return sorted(range(1, count), key=lambda step: -min(step, count - step))
+
+    def sent(self, half, phase, step):
         if (half + phase) % 2 == 0:
-            x, y = lax.rem(self.x + step + self.nx, self.nx), self.y
+            other = self.y * self.nx + lax.rem(self.x + step, self.nx)
         else:
-            x, y = self.x, lax.rem(self.y + step + self.ny, self.ny)
-        return {"ep": self.ep, "tp": y * self.nx + x}
-
-    def sent(self, half, phase, kind):
-        part = self.half // 2
-        step, begin, count, to = (
-            (0, 0, 2 * part, 1),
-            (0, 0, 2 * part, -1),
-            (-1, 0, part, 1),
-            (1, part, part, -1),
-        )[kind]
-        block = self.block(half, phase, step, begin, count)
-        at = (half * 2 + phase) * 4 + kind
+            other = lax.rem(self.y + step, self.ny) * self.nx + self.x
+        block = self.block(half, phase, 0)
+        at = (half * 2 + phase) * 4 + step
         return pltpu.make_async_remote_copy(
             src_ref=block,
             dst_ref=block,
             send_sem=self.send_sem.at[at],
             recv_sem=self.recv_sem.at[at],
-            device_id=self.other(half, phase, to),
+            device_id={"ep": self.ep, "tp": other},
             device_id_type=MESH,
         )
 
-    def arrived(self, half, phase, kind):
-        part = self.half // 2
-        step, begin, count = (
-            (-1, 0, 2 * part),
-            (1, 0, 2 * part),
-            (-2, 0, part),
-            (2, part, part),
-        )[kind]
-        block = self.block(half, phase, step, begin, count)
-        at = (half * 2 + phase) * 4 + kind
-        pltpu.make_async_copy(block, block, self.recv_sem.at[at]).wait()
-
     def start(self, half, phase):
-        self.sent(half, phase, 0).start()
-        self.sent(half, phase, 1).start()
-
-    def forward(self, half, phase):
-        self.arrived(half, phase, 0)
-        self.sent(half, phase, 2).start()
-        self.arrived(half, phase, 1)
-        self.sent(half, phase, 3).start()
+        for step in self.steps(half, phase):
+            self.sent(half, phase, step).start()
 
     def finish(self, half, phase):
-        self.arrived(half, phase, 2)
-        self.arrived(half, phase, 3)
+        for step in reversed(self.steps(half, phase)):
+            wait_for(self.block(half, phase, -step), self.recv_sem.at[(half * 2 + phase) * 4 + step])
+
+    def begin(self):
+        self.start(0, 0)
+        self.start(1, 0)
+
+    def turn(self):
+        for half in range(2):
+            self.finish(half, 0)
+            self.start(half, 1)
+
+    def end(self):
+        self.finish(0, 1)
+        self.finish(1, 1)
 
     def drain(self):
         for half in range(2):
             for phase in range(2):
-                for kind in range(4):
-                    self.sent(half, phase, kind).wait_send()
+                for step in self.steps(half, phase):
+                    self.sent(half, phase, step).wait_send()
+
+
+class Direct:
+    def __init__(self, buf, send_sem, recv_sem, place, ny, nx):
+        self.buf, self.send_sem, self.recv_sem = buf, send_sem, recv_sem
+        self.ep, self.y, self.x = place
+        self.ny, self.nx = ny, nx
+
+    def begin(self):
+        ny, nx = self.ny, self.nx
+        own = self.buf.at[self.y * nx + self.x]
+
+        def send(at, carry):
+            to_y = lax.rem(self.y + at // nx + ny // 2, ny)
+            to_x = lax.rem(self.x + lax.rem(at, nx) + nx // 2, nx)
+            pltpu.make_async_remote_copy(
+                src_ref=own,
+                dst_ref=own,
+                send_sem=self.send_sem,
+                recv_sem=self.recv_sem,
+                device_id={"ep": self.ep, "tp": to_y * nx + to_x},
+                device_id_type=MESH,
+            ).start()
+            return carry
+
+        self_at = (ny - ny // 2) * nx + (nx - nx // 2)
+        lax.fori_loop(0, self_at, send, 0)
+        lax.fori_loop(self_at + 1, ny * nx, send, 0)
+
+    def others(self):
+        return self.buf.at[pl.ds(0, self.ny * self.nx - 1)]
+
+    def end(self):
+        wait_for(self.others(), self.recv_sem)
+
+    def drain(self):
+        wait_for(self.others(), self.send_sem)
+
+
+def step_of(at, n_ep):
+    odd = lax.rem(at, 2)
+    return odd * ((at + 1) // 2) + (1 - odd) * lax.rem(n_ep - at // 2, n_ep)
 
 
 def wait_for(ref, sem):
@@ -250,52 +282,40 @@
     n_y,
     n_x,
     group,
-    recept_ref,
-    key_ref,
-    value_ref,
-    fix_ref,
-    fade_ref,
-    erase_ref,
-    speeds_ref,
-    gain_ref,
-    merge_hbm,
-    rows_ref,
-    scale_ref,
-    picks_ref,
-    share_ref,
-    gate_hbm,
-    up_hbm,
-    down_hbm,
-    blend_out,
-    expert_out,
-    merge_ref,
-    gate_up_ref,
-    down_ref,
-    send_buf,
-    recv_buf,
-    rows_all,
-    hidden_all,
-    back_buf,
-    ret_buf,
-    mixed_all,
-    pair_buf,
-    pair_in,
-    chip_pairs,
-    group_pairs,
-    state_out,
-    state_in,
-    load_sem,
-    ep_send,
-    ep_recv,
-    x_send,
-    x_recv,
-    h_send,
-    h_recv,
-    m_send,
-    m_recv,
-    scan_send,
-    scan_recv,
+    *refs,
 ):
+    hbm, refs = refs[:16], refs[16:]
+    blend_out, expert_out, *refs = refs
+    held, refs = refs[:14], refs[14:]
+    recept_ref, key_ref, value_ref, fix_ref, fade_ref, erase_ref, speeds_ref, gain_ref = held[:8]
+    merge_ref, rows_ref, scale_ref, picks_ref, share_ref, gate_up_ref = held[8:]
+    (
+        down_ref,
+        send_buf,
+        recv_buf,
+        rows_all,
+        hidden_all,
+        back_buf,
+        ret_buf,
+        mixed_all,
+        pair_buf,
+        pair_in,
+        chip_pairs,
+        group_pairs,
+        state_out,
+        state_in,
+        load_sem,
+        ep_send,
+        ep_recv,
+        x_send,
+        x_recv,
+        h_send,
+        h_recv,
+        m_send,
+        m_recv,
+        scan_send,
+        scan_recv,
+    ) = refs
     ep, tp = lax.axis_index("ep"), lax.axis_index("tp")
     core, z = lax.rem(ep, 2), ep // 2
     y, x = tp // n_x, lax.rem(tp, n_x)
@@ -307,16 +327,8 @@
     n_rows = rows_ref.shape[0]
     lanes = send_buf.shape[2]
     slots = n_ep * SLOTS
-    depth = gate_hbm.shape[1]
-
-    loads = [
-        pltpu.make_async_copy(gate_hbm, gate_up_ref.at[:, pl.ds(0, depth)], load_sem.at[0]),
-        pltpu.make_async_copy(up_hbm, gate_up_ref.at[:, pl.ds(depth, depth)], load_sem.at[1]),
-        pltpu.make_async_copy(down_hbm, down_ref, load_sem.at[2]),
-        pltpu.make_async_copy(merge_hbm, merge_ref, load_sem.at[3]),
-    ]
-    for load in loads:
-        load.start()
+    part = n_ep // CHUNKS
+    depth = hbm[13].shape[1]
 
     barrier = pltpu.get_barrier_semaphore()
 
@@ -330,31 +342,47 @@
         return carry
 
     lax.fori_loop(1, n_ep, greet, 0)
-    for step in (1, -1):
-        for other in (
-            y * n_x + lax.rem(x + step + n_x, n_x),
-            lax.rem(y + step + n_y, n_y) * n_x + x,
-        ):
-            pl.semaphore_signal(
-                barrier, inc=1, device_id={"ep": ep, "tp": other}, device_id_type=MESH
-            )
+
+    def greet_tp(step, carry):
+        pl.semaphore_signal(
+            barrier,
+            inc=1,
+            device_id={"ep": ep, "tp": lax.rem(tp + step, n_y * n_x)},
+            device_id_type=MESH,
+        )
+        return carry
+
+    lax.fori_loop(1, n_y * n_x, greet_tp, 0)
+
+    wide = [gate_up_ref.at[:, pl.ds(0, depth)], gate_up_ref.at[:, pl.ds(depth, depth)], down_ref]
+    targets = [*held[:13], *wide]
+    loads = [
+        pltpu.make_async_copy(hbm[at], targets[at], load_sem.at[at]) for at in range(len(targets))
+    ]
+    order = (9, 11, 10, 12, *range(8), 13, 14, 15, 8)
+    for at in order:
+        loads[at].start()
+    for at in order[:4]:
+        loads[at].wait()
 
     widened = rows_ref[...].astype(F32)
     strength = lax.rsqrt(jnp.mean(widened * widened, axis=1, keepdims=True) + 1e-6)
     own = pl.ds(pl.multiple_of(tp * lanes, 128), lanes)
     normed = (rows_ref[:, own].astype(F32) * strength * scale_ref[:, own]).astype(BF16)
-    slot = iota((n_rows, slots), 1)
-    expert = slot // SLOTS
-    named = [picks_ref[:, k : k + 1] == expert for k in range(2)]
+    slot = iota((slots, n_rows), 0)
+    expert = lax.rem(step_of(slot // SLOTS, n_ep) + ep, n_ep)
+    named = [picks_ref[k : k + 1, :] == expert for k in range(2)]
     either = named[0] | named[1]
-    earlier = chosen(iota((n_rows, n_rows), 1) < iota((n_rows, n_rows), 0))
-    rank = dot(earlier, chosen(either), 1, 0)
+    earlier = chosen(iota((n_rows, n_rows), 0) < iota((n_rows, n_rows), 1))
+    rank = dot(chosen(either), earlier, 1, 0)
     taken = either & (rank == lax.rem(slot, SLOTS).astype(F32))
-    weight = jnp.where(taken & named[0], share_ref[:, 0:1], 0.0) + jnp.where(
-        taken & named[1], share_ref[:, 1:2], 0.0
+    weight = jnp.where(taken & named[0], share_ref[0:1, :], 0.0) + jnp.where(
+        taken & named[1], share_ref[1:2, :], 0.0
     )
-    send_buf[...] = dot(chosen(taken), normed, 0, 0).reshape(n_ep, SLOTS, lanes).astype(BF16)
-
+    send_buf[...] = dot(chosen(taken), normed, 1, 0).reshape(n_ep, SLOTS, lanes).astype(BF16)
+
+    for at in range(8):
+        loads[at].wait()
     matrices = pair_matrices(
         recept_ref[...],
         key_ref[...],
@@ -365,28 +393,36 @@
         speeds_ref[...],
     )
 
-    pl.semaphore_wait(barrier, n_ep - 1 + 4)
-
-    def ep_copy(src, dst, step, at):
-        other = lax.rem(ep + step, n_ep)
+    pl.semaphore_wait(barrier, n_ep - 1 + n_y * n_x - 1)
+
+    def ep_copy(src, dst, at, turn, sems):
+        step = step_of(at, n_ep)
         return pltpu.make_async_remote_copy(
-            src_ref=src.at[other],
-            dst_ref=dst.at[ep],
-            send_sem=ep_send.at[at],
-            recv_sem=ep_recv.at[at],
-            device_id={"ep": other, "tp": tp},
+            src_ref=src.at[at, pl.ds(0, CAP)],
+            dst_ref=dst.at[at, pl.ds(0, CAP)],
+            send_sem=ep_send.at[sems],
+            recv_sem=ep_recv.at[sems],
+            device_id={"ep": lax.rem(ep + turn * step + n_ep, n_ep), "tp": tp},
             device_id_type=MESH,
         )
 
-    def ep_exchange(src, dst, at):
-        def send(step, carry):
-            ep_copy(src, dst, step, at).start()
+    def ep_exchange(src, dst, chunk, turn, sems):
+        begin, end = max(1, chunk * part), (chunk + 1) * part
+
+        def send(at, carry):
+            ep_copy(src, dst, begin + end - 1 - at, turn, sems).start()
             return carry
 
-        lax.fori_loop(1, n_ep, send, 0)
-        dst[ep] = src[ep]
-
-    ep_exchange(send_buf, recv_buf, 0)
+        lax.fori_loop(begin, end, send, 0)
+        if chunk == 0:
+            dst[0] = src[0]
+
+    def ep_bytes(buf, chunk):
+        begin = max(1, chunk * part)
+        return buf.at[pl.ds(begin, (chunk + 1) * part - begin), pl.ds(0, CAP)]
+
+    for chunk in reversed(range(CHUNKS)):
+        ep_exchange(send_buf, recv_buf, chunk, 1, chunk)
 
     carried, own_out, pair = pair_results(*matrices)
     pair_buf[...] = pair
@@ -423,6 +459,54 @@
             )
         )
         local[-1].start()
+    blank = lax.rem(iota((part * SLOTS, lanes), 0), SLOTS) >= CAP
+    packed, spread = iota((part * CAP, part * SLOTS), 0), iota((part * CAP, part * SLOTS), 1)
+    inner = lax.rem(spread, SLOTS)
+    pack = chosen((inner < CAP) & (spread // SLOTS * CAP + inner == packed))
+
+    spot = (ep, y, x)
+    size = n_y * n_x
+    xs = [
+        TwoPhase(rows_all.at[k], x_send.at[k], x_recv.at[k], spot, n_y, n_x) for k in range(CHUNKS)
+    ]
+    hs = [
+        Direct(hidden_all.at[k], h_send.at[k], h_recv.at[k], spot, n_y, n_x) for k in range(CHUNKS)
+    ]
+    ms = Direct(mixed_all, m_send.at[0], m_recv.at[0], spot, n_y, n_x)
+
+    def live(buf, chunk):
+        block = buf[chunk * part : (chunk + 1) * part].astype(F32).reshape(part * SLOTS, lanes)
+        return jnp.where(blank, 0.0, block).astype(BF16)
+
+    def arrive(chunk):
+        wait_for(ep_bytes(recv_buf, chunk), ep_recv.at[chunk])
+        rows_all[chunk, y, x] = dot(pack, live(recv_buf, chunk), 1, 0).astype(BF16)
+
+    def gate_up(chunk):
+        total = jnp.zeros((part * CAP, 2 * depth), F32)
+        for j in range(size):
+            total = total + dot(
+                rows_all[chunk, j // n_x, j % n_x],
+                gate_up_ref[j * lanes : (j + 1) * lanes, :],
+                1,
+                0,
+            )
+        gated, raised = total[:, :depth], total[:, depth:]
+        hidden_all[chunk, tp] = (gated / (1.0 + jnp.exp(-gated)) * raised).astype(BF16)
+
+    def lower(chunk):
+        result = jnp.zeros((part * CAP, lanes), F32)
+        for j in range(size):
+            result = result + dot(
+                hidden_all[chunk, j], down_ref[j * depth : (j + 1) * depth, :], 1, 0
+            )
+        spread_out = dot(pack, result.astype(BF16), 0, 0).reshape(part, SLOTS, lanes)
+        back_buf[chunk * part : (chunk + 1) * part] = spread_out.astype(BF16)
+        ep_exchange(back_buf, ret_buf, chunk, -1, CHUNKS + chunk)
+
+    arrive(0)
+    xs[0].begin()
+    xs[0].turn()
     for step in range(1, group):
         at = lax.rem(place - step + group, group)
         wait_for(chip_pairs.at[at], scan_recv.at[step])
@@ -449,26 +533,14 @@
         def _(step=step):
             group_copy(step).start()
 
-    wait_for(recv_buf.at[pl.ds(0, n_ep - 1)], ep_recv.at[0])
-    packed, spread = iota((n_ep * CAP, slots), 0), iota((n_ep * CAP, slots), 1)
-    inner = lax.rem(spread, SLOTS)
-    pack = chosen((inner < CAP) & (spread // SLOTS * CAP + inner == packed))
-    arrived = recv_buf[...].astype(F32).reshape(slots, lanes).astype(BF16)
-    rows_all[y, x] = dot(pack, arrived, 1, 0).astype(BF16)
-
-    spot = (ep, y, x)
-    xs = Gather(rows_all, x_send, x_recv, spot, n_y, n_x)
-    hs = Gather(hidden_all, h_send, h_recv, spot, n_y, n_x)
-    ms = Gather(mixed_all, m_send, m_recv, spot, n_y, n_x)
-    both = (0, 1)
-    for half in both:
-        xs.start(half, 0)
-    for half in both:
-        xs.forward(half, 0)
-    for half in both:
-        xs.finish(half, 0)
-        xs.start(half, 1)
-
+    arrive(1)
+    xs[1].begin()
+    xs[1].turn()
+    xs[0].end()
+    for load in loads[13:15]:
+        load.wait()
+    gate_up(0)
+    hs[0].begin()
     for step in range(1, n_group):
 
         @pl.when(mine >= step)
@@ -484,10 +556,9 @@
     give = scan_copy(state_out, state_in, partner, group + n_group - 1)
     give.start()
     state_own = jnp.where(even, state_0, state_1)
-
-    for half in both:
-        xs.forward(half, 1)
-
+    xs[1].end()
+    gate_up(1)
+    hs[1].begin()
     give.wait_recv()
     state_other = state_in[...]
     state_a = jnp.where(even, state_own, state_other)
@@ -505,58 +576,21 @@
     centred = out - mean
     spread_of = by_head(*per_head(centred * centred), (n, c)) * (1.0 / HEAD)
     mixed = centred * lax.rsqrt(spread_of + 0.00064) * gain_ref[...]
-    mixed_all[y, x] = mixed.astype(BF16)
-    for half in both:
-        ms.start(half, 0)
-
-    for half in both:
-        xs.finish(half, 1)
-    for load in loads[:2]:
-        load.wait()
-
-    total = jnp.zeros((n_ep * CAP, 2 * depth), F32)
-    for j in range(n_y * n_x):
-        total = total + dot(
-            rows_all[j // n_x, j % n_x], gate_up_ref[j * lanes : (j + 1) * lanes, :], 1, 0
-        )
-    gated, raised = total[:, :depth], total[:, depth:]
-    hidden_all[y, x] = (gated / (1.0 + jnp.exp(-gated)) * raised).astype(BF16)
-    for half in both:
-        hs.start(half, 0)
-    for half in both:
-        ms.forward(half, 0)
-    for half in both:
-        hs.forward(half, 0)
-    for half in both:
-        hs.finish(half, 0)
-        hs.start(half, 1)
-    for half in both:
-        ms.finish(half, 0)
-        ms.start(half, 1)
-    for half in both:
-        hs.forward(half, 1)
-    for half in both:
-        ms.forward(half, 1)
-    for half in both:
-        hs.finish(half, 1)
-    loads[2].wait()
-    result = jnp.zeros((n_ep * CAP, lanes), F32)
-    for j in range(n_y * n_x):
-        result = result + dot(
-            hidden_all[j // n_x, j % n_x], down_ref[j * depth : (j + 1) * depth, :], 1, 0
-        )
-    back_buf[...] = dot(pack, result.astype(BF16), 0, 0).reshape(n_ep, SLOTS, lanes).astype(BF16)
-    ep_exchange(back_buf, ret_buf, 1)
-
-    for half in both:
-        ms.finish(half, 1)
-    loads[3].wait()
+    mixed_all[tp] = mixed.astype(BF16)
+    ms.begin()
+    hs[0].end()
+    loads[15].wait()
+    lower(0)
+    hs[1].end()
+    lower(1)
+    ms.end()
+    loads[8].wait()
     blend = jnp.zeros(blend_out.shape, F32)
-    for j in range(n_y * n_x):
-        blend = blend + dot(mixed_all[j // n_x, j % n_x], merge_ref[j * c : (j + 1) * c, :], 1, 0)
+    for j in range(size):
+        blend = blend + dot(mixed_all[j], merge_ref[j * c : (j + 1) * c, :], 1, 0)
     blend_out[...] = blend.astype(BF16)
 
-    for gather in (xs, hs, ms):
+    for gather in (*xs, *hs, ms):
         gather.drain()
     swap.wait_send()
     give.wait_send()
@@ -568,12 +602,18 @@
         def _(step=step):
             group_copy(step).wait_send()
 
-    wait_for(send_buf.at[pl.ds(0, n_ep - 1)], ep_send.at[0])
-    wait_for(ret_buf.at[pl.ds(0, n_ep - 1)], ep_recv.at[1])
-    returned = ret_buf[...].astype(F32).reshape(slots, lanes).astype(BF16)
+    for chunk in range(CHUNKS):
+        wait_for(ep_bytes(send_buf, chunk), ep_send.at[chunk])
     w_hi, w_lo = split(weight)
-    expert_out[...] = (dot(w_hi, returned, 1, 0) + dot(w_lo, returned, 1, 0)).astype(BF16)
-    wait_for(back_buf.at[pl.ds(0, n_ep - 1)], ep_send.at[1])
+    share = jnp.zeros(expert_out.shape, F32)
+    for chunk in range(CHUNKS):
+        wait_for(ep_bytes(ret_buf, chunk), ep_recv.at[CHUNKS + chunk])
+        returned = live(ret_buf, chunk)
+        span = slice(chunk * part * SLOTS, (chunk + 1) * part * SLOTS)
+        share = share + (dot(w_hi[span], returned, 0, 0) + dot(w_lo[span], returned, 0, 0))
+    expert_out[...] = share.astype(BF16)
+    for chunk in range(CHUNKS):
+        wait_for(ep_bytes(back_buf, chunk), ep_send.at[CHUNKS + chunk])
 
 
 def body(
@@ -602,10 +642,12 @@
     n_rows, width = rows.shape
     lanes = down.shape[2]
     depth = gate.shape[2]
-    slots = n_ep * CAP
+    chunk_rows = n_ep // CHUNKS * CAP
     n_group = n_ep // 2 // group
     scans = group + n_group
     vmem, hbm = pl.BlockSpec(memory_space=pltpu.VMEM), pl.BlockSpec(memory_space=pltpu.HBM)
+    small = (recept, key, value, fix, fade, erase, speeds, gain.reshape(1, c), merge, rows)
+    small = (*small, scale.reshape(1, width), picks.T, share.T)
     dma = pltpu.SemaphoreType.DMA
     return pl.pallas_call(
         lambda *refs: kernel(n_ep, n_y, n_x, group, *refs),
@@ -613,58 +655,41 @@
             jax.ShapeDtypeStruct((n, merge.shape[1]), BF16),
             jax.ShapeDtypeStruct((n_rows, lanes), BF16),
         ),
-        in_specs=[vmem] * 8 + [hbm] + [vmem] * 4 + [hbm] * 3,
+        in_specs=[hbm] * 16,
         out_specs=(vmem, vmem),
         scratch_shapes=[
-            pltpu.VMEM(merge.shape, BF16),
+            *(pltpu.VMEM(array.shape, array.dtype) for array in small),
             pltpu.VMEM((width, 2 * depth), BF16),
             pltpu.VMEM(down.shape[1:], BF16),
             pltpu.VMEM((n_ep, SLOTS, lanes), BF16),
             pltpu.VMEM((n_ep, SLOTS, lanes), BF16),
-            pltpu.VMEM((n_y, n_x, slots, lanes), BF16),
-            pltpu.VMEM((n_y, n_x, slots, depth), BF16),
+            pltpu.VMEM((CHUNKS, n_y, n_x, chunk_rows, lanes), BF16),
+            pltpu.VMEM((CHUNKS, n_y * n_x, chunk_rows, depth), BF16),
             pltpu.VMEM((n_ep, SLOTS, lanes), BF16),
             pltpu.VMEM((n_ep, SLOTS, lanes), BF16),
-            pltpu.VMEM((n_y, n_x, n, c), BF16),
+            pltpu.VMEM((n_y * n_x, n, c), BF16),
             pltpu.VMEM((n, c), F32),
             pltpu.VMEM((HEAD, c), F32),
             pltpu.VMEM((group, HEAD, c), F32),
             pltpu.VMEM((n_group, HEAD, c), F32),
             pltpu.VMEM((HEAD, c), F32),
             pltpu.VMEM((HEAD, c), F32),
-            dma((4,)),
-            dma((2,)),
-            dma((2,)),
             dma((16,)),
-            dma((16,)),
-            dma((16,)),
-            dma((16,)),
-            dma((16,)),
-            dma((16,)),
+            dma((2 * CHUNKS,)),
+            dma((2 * CHUNKS,)),
+            dma((CHUNKS, 16)),
+            dma((CHUNKS, 16)),
+            dma((CHUNKS,)),
+            dma((CHUNKS,)),
+            dma((1,)),
+            dma((1,)),
             dma((scans,)),
             dma((scans,)),
         ],
         compiler_params=pltpu.CompilerParams(
             collective_id=0, has_side_effects=True, vmem_limit_bytes=56 << 20
         ),
-    )(
-        recept,
-        key,
-        value,
-        fix,
-        fade,
-        erase,
-        speeds,
-        gain.reshape(1, c),
-        merge,
-        rows,
-        scale.reshape(1, width),
-        picks,
-        share,
-        gate[0],
-        up[0],
-        down[0],
-    )
+    )(*small, gate[0], up[0], down[0])
 
 
 def solution(mesh):

time: 80.2 us -> 66.3 us (0.83)
  Pallas kernels: 75.2 us -> 63.4 us
  local copies, waits for them, and re-layouts: 4.19 us -> 2.1 us
    pallas_call x1, Pallas kernels: 75.2 us -> 63.4 us  [body(): pl.pallas_call(lambda *refs: kernel(n_ep, n_y, n_x, group, *refs), out_sh...]
    unnamed x10 -> x4, local copies, waits for them, and re-layouts: 4.19 us -> 2.1 us
where the time goes in v2:
time: 66.3 us; the launch traced here: 66.2 us
  Pallas kernels  63.4 us (96%)
  local copies, waits for them, and re-layouts  2.1 us (3%)
    pallas_call x1, Pallas kernels, body(): pl.pallas_call(lambda *refs: kernel(n_ep, n_y, n_x, group, *refs), out_sh...  63.4 us
    unnamed x4, local copies, waits for them, and re-layouts  2.1 us

profile of v2, /device:TPU:1, one launch (start us, length us, event | category | flops | bytes accessed | tf_op | source)
XLA Modules:
  0.0 66.2 jit_solution(4408084779306957681)
XLA Ops:
  0.6 63.4 %shard_map.167 = (bf16[128,256]{1,0:T(8,128)(2,1)}, bf16[64,256]{1,0:T(8,128)(2,1)}) custom-call(bf16[128,128]{1,0:T(8,128)(2,1)} %refs_0_.1, bf16[128,128]{1,0:T(8,128)(2,1)} %refs_1_.1, bf16[128,128]{1,0:T(8,128)(2,1)} %refs_2_.1, bf16[128,128]{1,0:T(8,128)(2,1)} %refs_3_.1, bf16[128,128]{1,0:T(8,128)(2,1)} %refs_4_.1, bf16[128,128]{1,0:T(8,128)(2,1)} %refs_5_.1, ...), custom_call_target="tpu_custom_call" | custom-call | tf_op jit(solution)/shard_map/pallas_call | solution.py:652
  64.0 0.0 copy-start
  64.1 1.5 %copy.20 = bf16[128,256]{1,0:T(8,128)(2,1)} copy(bf16[128,256]{1,0:T(8,128)(2,1)} %get-tuple-element.4) | data formatting | bytes 131072
  65.5 0.0 copy-done
  65.5 0.6 copy.21
Async XLA Ops:
  64.0 1.5 %copy-start = (bf16[64,256]{1,0:T(8,128)(2,1)S(1)}, bf16[64,256]{1,0:T(8,128)(2,1)}, u32[]{:S(2)}) copy-start(bf16[64,256]{1,0:T(8,128)(2,1)} %get-tuple-element.5) | copy-start | bytes 98308

commit v3 on v2

--- a/solution.py
+++ b/solution.py
@@ -171,64 +171,63 @@
         self.ny, self.nx = ny, nx
         self.half = buf.shape[2] // 2
 
-    def block(self, half, phase, step):
-        rows = pl.ds(half * self.half, self.half)
-        if (half + phase) % 2 == 0:
-            at = lax.rem(self.x + step + self.nx, self.nx)
-            if phase == 0:
-                return self.buf.at[self.y, at, rows]
-            return self.buf.at[:, at, rows]
-        at = lax.rem(self.y + step + self.ny, self.ny)
-        if phase == 0:
-            return self.buf.at[at, self.x, rows]
-        return self.buf.at[at, :, rows]
+    def along_x(self, half, phase):
+        return (half + phase) % 2 == 0
+
+    def rows(self, half):
+        return pl.ds(half * self.half, self.half)
+
+    def moved(self, half, phase, step):
+        if self.along_x(half, phase):
+            return self.y, lax.rem(self.x + step + self.nx, self.nx)
+        return lax.rem(self.y + step + self.ny, self.ny), self.x
 
     def steps(self, half, phase):
-        count = self.nx if (half + phase) % 2 == 0 else self.ny
+        count = self.nx if self.along_x(half, phase) else self.ny
         return sorted(range(1, count), key=lambda step: -min(step, count - step))
 
-    def sent(self, half, phase, step):
-        if (half + phase) % 2 == 0:
-            other = self.y * self.nx + lax.rem(self.x + step, self.nx)
-        else:
-            other = lax.rem(self.y + step, self.ny) * self.nx + self.x
-        block = self.block(half, phase, 0)
-        at = (half * 2 + phase) * 4 + step
-        return pltpu.make_async_remote_copy(
-            src_ref=block,
-            dst_ref=block,
-            send_sem=self.send_sem.at[at],
-            recv_sem=self.recv_sem.at[at],
-            device_id={"ep": self.ep, "tp": other},
+    def send(self, half, phase, block, step, out, into):
+        at = self.buf.at[block[0], block[1], self.rows(half)]
+        to_y, to_x = self.moved(half, phase, step)
+        pltpu.make_async_remote_copy(
+            src_ref=at,
+            dst_ref=at,
+            send_sem=self.send_sem.at[half * 2 + out],
+            recv_sem=self.recv_sem.at[half * 4 + into],
+            device_id={"ep": self.ep, "tp": to_y * self.nx + to_x},
             device_id_type=MESH,
-        )
-
-    def start(self, half, phase):
-        for step in self.steps(half, phase):
-            self.sent(half, phase, step).start()
-
-    def finish(self, half, phase):
-        for step in reversed(self.steps(half, phase)):
-            wait_for(self.block(half, phase, -step), self.recv_sem.at[(half * 2 + phase) * 4 + step])
+        ).start()
 
     def begin(self):
-        self.start(0, 0)
-        self.start(1, 0)
+        own = (self.y, self.x)
+        for half in range(2):
+            for step in self.steps(half, 0):
+                self.send(half, 0, own, step, 0, step)
+        for half in range(2):
+            for step in self.steps(half, 1):
+                self.send(half, 1, own, step, 0, 0)
 
     def turn(self):
+        for index in range(3):
+            for half in range(2):
+                step = self.steps(half, 0)[2 - index]
+                block = self.moved(half, 0, -step)
+                at = self.buf.at[block[0], block[1], self.rows(half)]
+                wait_for(at, self.recv_sem.at[half * 4 + step])
+                for to in self.steps(half, 1):
+                    self.send(half, 1, block, to, 1, 0)
+
+    def blocks(self, half, count_y, count_x):
+        return self.buf.at[pl.ds(0, count_y), pl.ds(0, count_x), self.rows(half)]
+
+    def end(self):
         for half in range(2):
-            self.finish(half, 0)
-            self.start(half, 1)
-
-    def end(self):
-        self.finish(0, 1)
-        self.finish(1, 1)
+            wait_for(self.blocks(half, 3, 4), self.recv_sem.at[half * 4])
 
     def drain(self):
         for half in range(2):
-            for phase in range(2):
-                for step in self.steps(half, phase):
-                    self.sent(half, phase, step).wait_send()
+            wait_for(self.blocks(half, 2, 3), self.send_sem.at[half * 2])
+            wait_for(self.blocks(half, 3, 3), self.send_sem.at[half * 2 + 1])
 
 
 class Direct:
@@ -332,27 +331,15 @@
 
     barrier = pltpu.get_barrier_semaphore()
 
-    def greet(step, carry):
+    def greet(at_ep, at_tp):
         pl.semaphore_signal(
-            barrier,
-            inc=1,
-            device_id={"ep": lax.rem(ep + step, n_ep), "tp": tp},
-            device_id_type=MESH,
+            barrier, inc=1, device_id={"ep": at_ep, "tp": at_tp}, device_id_type=MESH
         )
-        return carry
-
-    lax.fori_loop(1, n_ep, greet, 0)
-
-    def greet_tp(step, carry):
-        pl.semaphore_signal(
-            barrier,
-            inc=1,
-            device_id={"ep": ep, "tp": lax.rem(tp + step, n_y * n_x)},
-            device_id_type=MESH,
-        )
-        return carry
-
-    lax.fori_loop(1, n_y * n_x, greet_tp, 0)
+
+    for step in sorted(range(1, n_ep), key=lambda step: -min(step, n_ep - step)):
+        greet(lax.rem(ep + step, n_ep), tp)
+    for step in range(1, n_y * n_x):
+        greet(ep, lax.rem(tp + step, n_y * n_x))
 
     wide = [gate_up_ref.at[:, pl.ds(0, depth)], gate_up_ref.at[:, pl.ds(depth, depth)], down_ref]
     targets = [*held[:13], *wide]
@@ -421,8 +408,52 @@
         begin = max(1, chunk * part)
         return buf.at[pl.ds(begin, (chunk + 1) * part - begin), pl.ds(0, CAP)]
 
-    for chunk in reversed(range(CHUNKS)):
+    for chunk in range(CHUNKS):
         ep_exchange(send_buf, recv_buf, chunk, 1, chunk)
+
+    blank = lax.rem(iota((part * SLOTS, lanes), 0), SLOTS) >= CAP
+    packed, spread = iota((part * CAP, part * SLOTS), 0), iota((part * CAP, part * SLOTS), 1)
+    inner = lax.rem(spread, SLOTS)
+    pack = chosen((inner < CAP) & (spread // SLOTS * CAP + inner == packed))
+
+    spot = (ep, y, x)
+    size = n_y * n_x
+    xs = [
+        TwoPhase(rows_all.at[k], x_send.at[k], x_recv.at[k], spot, n_y, n_x) for k in range(CHUNKS)
+    ]
+    hs = [
+        Direct(hidden_all.at[k], h_send.at[k], h_recv.at[k], spot, n_y, n_x) for k in range(CHUNKS)
+    ]
+    ms = TwoPhase(mixed_all, m_send, m_recv, spot, n_y, n_x)
+
+    def live(buf, chunk):
+        block = buf[chunk * part : (chunk + 1) * part].astype(F32).reshape(part * SLOTS, lanes)
+        return jnp.where(blank, 0.0, block).astype(BF16)
+
+    def arrive(chunk):
+        wait_for(ep_bytes(recv_buf, chunk), ep_recv.at[chunk])
+        rows_all[chunk, y, x] = dot(pack, live(recv_buf, chunk), 1, 0).astype(BF16)
+
+    def gate_up(chunk):
+        total = jnp.zeros((part * CAP, 2 * depth), F32)
+        for j in range(size):
+            total = total + dot(
+                rows_all[chunk, j // n_x, j % n_x],
+                gate_up_ref[j * lanes : (j + 1) * lanes, :],
+                1,
+                0,
+            )
+        gated, raised = total[:, :depth], total[:, depth:]
+        hidden_all[chunk, tp] = (gated / (1.0 + jnp.exp(-gated)) * raised).astype(BF16)
+
+    def lower(chunk):
+        result = jnp.zeros((part * CAP, lanes), F32)
+        for j in range(0, size, 2):
+            left = jnp.concatenate([hidden_all[chunk, j], hidden_all[chunk, j + 1]], 1)
+            result = result + dot(left, down_ref[j * depth : (j + 2) * depth, :], 1, 0)
+        spread_out = dot(pack, result.astype(BF16), 0, 0).reshape(part, SLOTS, lanes)
+        back_buf[chunk * part : (chunk + 1) * part] = spread_out.astype(BF16)
+        ep_exchange(back_buf, ret_buf, chunk, -1, CHUNKS + chunk)
 
     carried, own_out, pair = pair_results(*matrices)
     pair_buf[...] = pair
@@ -440,6 +471,8 @@
     theirs = pair_buf.at[pl.ds(pl.multiple_of(HEAD * (1 - core), HEAD), HEAD)]
     swap = scan_copy(theirs, pair_in, partner, 0)
     swap.start()
+    arrive(0)
+    xs[0].begin()
     swap.wait_recv()
     own_pair = pair_buf[pl.ds(pl.multiple_of(HEAD * core, HEAD), HEAD), :]
     other_pair = pair_in[...]
@@ -459,54 +492,9 @@
             )
         )
         local[-1].start()
-    blank = lax.rem(iota((part * SLOTS, lanes), 0), SLOTS) >= CAP
-    packed, spread = iota((part * CAP, part * SLOTS), 0), iota((part * CAP, part * SLOTS), 1)
-    inner = lax.rem(spread, SLOTS)
-    pack = chosen((inner < CAP) & (spread // SLOTS * CAP + inner == packed))
-
-    spot = (ep, y, x)
-    size = n_y * n_x
-    xs = [
-        TwoPhase(rows_all.at[k], x_send.at[k], x_recv.at[k], spot, n_y, n_x) for k in range(CHUNKS)
-    ]
-    hs = [
-        Direct(hidden_all.at[k], h_send.at[k], h_recv.at[k], spot, n_y, n_x) for k in range(CHUNKS)
-    ]
-    ms = Direct(mixed_all, m_send.at[0], m_recv.at[0], spot, n_y, n_x)
-
-    def live(buf, chunk):
-        block = buf[chunk * part : (chunk + 1) * part].astype(F32).reshape(part * SLOTS, lanes)
-        return jnp.where(blank, 0.0, block).astype(BF16)
-
-    def arrive(chunk):
-        wait_for(ep_bytes(recv_buf, chunk), ep_recv.at[chunk])
-        rows_all[chunk, y, x] = dot(pack, live(recv_buf, chunk), 1, 0).astype(BF16)
-
-    def gate_up(chunk):
-        total = jnp.zeros((part * CAP, 2 * depth), F32)
-        for j in range(size):
-            total = total + dot(
-                rows_all[chunk, j // n_x, j % n_x],
-                gate_up_ref[j * lanes : (j + 1) * lanes, :],
-                1,
-                0,
-            )
-        gated, raised = total[:, :depth], total[:, depth:]
-        hidden_all[chunk, tp] = (gated / (1.0 + jnp.exp(-gated)) * raised).astype(BF16)
-
-    def lower(chunk):
-        result = jnp.zeros((part * CAP, lanes), F32)
-        for j in range(size):
-            result = result + dot(
-                hidden_all[chunk, j], down_ref[j * depth : (j + 1) * depth, :], 1, 0
-            )
-        spread_out = dot(pack, result.astype(BF16), 0, 0).reshape(part, SLOTS, lanes)
-        back_buf[chunk * part : (chunk + 1) * part] = spread_out.astype(BF16)
-        ep_exchange(back_buf, ret_buf, chunk, -1, CHUNKS + chunk)
-
-    arrive(0)
-    xs[0].begin()
     xs[0].turn()
+    arrive(1)
+    xs[1].begin()
     for step in range(1, group):
         at = lax.rem(place - step + group, group)
         wait_for(chip_pairs.at[at], scan_recv.at[step])
@@ -533,14 +521,15 @@
         def _(step=step):
             group_copy(step).start()
 
-    arrive(1)
-    xs[1].begin()
     xs[1].turn()
     xs[0].end()
     for load in loads[13:15]:
         load.wait()
     gate_up(0)
     hs[0].begin()
+    xs[1].end()
+    gate_up(1)
+    hs[1].begin()
     for step in range(1, n_group):
 
         @pl.when(mine >= step)
@@ -556,9 +545,9 @@
     give = scan_copy(state_out, state_in, partner, group + n_group - 1)
     give.start()
     state_own = jnp.where(even, state_0, state_1)
-    xs[1].end()
-    gate_up(1)
-    hs[1].begin()
+    hs[0].end()
+    loads[15].wait()
+    lower(0)
     give.wait_recv()
     state_other = state_in[...]
     state_a = jnp.where(even, state_own, state_other)
@@ -576,18 +565,18 @@
     centred = out - mean
     spread_of = by_head(*per_head(centred * centred), (n, c)) * (1.0 / HEAD)
     mixed = centred * lax.rsqrt(spread_of + 0.00064) * gain_ref[...]
-    mixed_all[tp] = mixed.astype(BF16)
+    mixed_all[y, x] = mixed.astype(BF16)
     ms.begin()
-    hs[0].end()
-    loads[15].wait()
-    lower(0)
     hs[1].end()
     lower(1)
+    ms.turn()
     ms.end()
     loads[8].wait()
     blend = jnp.zeros(blend_out.shape, F32)
-    for j in range(size):
-        blend = blend + dot(mixed_all[j], merge_ref[j * c : (j + 1) * c, :], 1, 0)
+    for j in range(0, size, 2):
+        at_y, at_x = j // n_x, j % n_x
+        left = jnp.concatenate([mixed_all[at_y, at_x], mixed_all[at_y, at_x + 1]], 1)
+        blend = blend + dot(left, merge_ref[j * c : (j + 2) * c, :], 1, 0)
     blend_out[...] = blend.astype(BF16)
 
     for gather in (*xs, *hs, ms):
@@ -652,8 +641,8 @@
     return pl.pallas_call(
         lambda *refs: kernel(n_ep, n_y, n_x, group, *refs),
         out_shape=(
-            jax.ShapeDtypeStruct((n, merge.shape[1]), BF16),
-            jax.ShapeDtypeStruct((n_rows, lanes), BF16),
+            pltpu.VMEM((n, merge.shape[1]), BF16),
+            pltpu.VMEM((n_rows, lanes), BF16),
         ),
         in_specs=[hbm] * 16,
         out_specs=(vmem, vmem),
@@ -667,7 +656,7 @@
             pltpu.VMEM((CHUNKS, n_y * n_x, chunk_rows, depth), BF16),
             pltpu.VMEM((n_ep, SLOTS, lanes), BF16),
             pltpu.VMEM((n_ep, SLOTS, lanes), BF16),
-            pltpu.VMEM((n_y * n_x, n, c), BF16),
+            pltpu.VMEM((n_y, n_x, n, c), BF16),
             pltpu.VMEM((n, c), F32),
             pltpu.VMEM((HEAD, c), F32),
             pltpu.VMEM((group, HEAD, c), F32),
@@ -677,12 +666,12 @@
             dma((16,)),
             dma((2 * CHUNKS,)),
             dma((2 * CHUNKS,)),
-            dma((CHUNKS, 16)),
-            dma((CHUNKS, 16)),
+            dma((CHUNKS, 4)),
+            dma((CHUNKS, 8)),
             dma((CHUNKS,)),
             dma((CHUNKS,)),
-            dma((1,)),
-            dma((1,)),
+            dma((4,)),
+            dma((8,)),
             dma((scans,)),
             dma((scans,)),
         ],

time: 66.3 us -> 57.7 us (0.87)
  Pallas kernels: 63.4 us -> 55.7 us
  local copies, waits for them, and re-layouts: 2.1 us -> 1.25 us
    pallas_call x1, Pallas kernels: 63.4 us -> 55.7 us  [body(): pl.pallas_call(lambda *refs: kernel(n_ep, n_y, n_x, group, *refs), out_sh...]
    unnamed x4 -> x2, local copies, waits for them, and re-layouts: 2.1 us -> 1.25 us
where the time goes in v3:
time: 57.7 us; the launch traced here: 57.6 us
  Pallas kernels  55.7 us (97%)
  local copies, waits for them, and re-layouts  1.25 us (2%)
  between operations  0.65 us (1%)
    pallas_call x1, Pallas kernels, body(): pl.pallas_call(lambda *refs: kernel(n_ep, n_y, n_x, group, *refs), out_sh...  55.7 us
    unnamed x2, local copies, waits for them, and re-layouts  1.25 us

profile of v3, /device:TPU:1, one launch (start us, length us, event | category | flops | bytes accessed | tf_op | source)
XLA Modules:
  0.0 57.6 jit_solution(14245303235220645171)
XLA Ops:
  0.6 55.7 %shard_map.167 = (bf16[128,256]{1,0:T(8,128)(2,1)S(1)}, bf16[64,256]{1,0:T(8,128)(2,1)S(1)}) custom-call(bf16[128,128]{1,0:T(8,128)(2,1)} %refs_0_.1, bf16[128,128]{1,0:T(8,128)(2,1)} %refs_1_.1, bf16[128,128]{1,0:T(8,128)(2,1)} %refs_2_.1, bf16[128,128]{1,0:T(8,128)(2,1)} %refs_3_.1, bf16[128,128]{1,0:T(8,128)(2,1)} %refs_4_.1, bf16[128,128]{1,0:T(8,128)(2,1)} %refs_5_.1, ...), custom_call_target="tpu_custom_call" | custom-call | tf_op jit(solution)/shard_map/pallas_call | solution.py:641
  56.3 0.6 %copy.20 = bf16[128,256]{1,0:T(8,128)(2,1)} copy(bf16[128,256]{1,0:T(8,128)(2,1)S(1)} %get-tuple-element.2) | data formatting | bytes 131072
  56.9 0.6 %copy.21 = bf16[64,256]{1,0:T(8,128)(2,1)} copy(bf16[64,256]{1,0:T(8,128)(2,1)S(1)} %get-tuple-element.3) | data formatting | bytes 65536
